TPU v7x, 32 devices: a whole 2x2x4 slice. The times are simulated.
32 devices in a mesh: ep: 8 (over z, core), tp: 4 (over y, x).
Axes of the slice: x: 2, y: 2, z: 4, core: 2. Of those that a mesh axis runs over, the one named last changes fastest.
Arguments:
- query_rows: bfloat16 [6144, 1024], P('ep', 'tp'), may hold values from -600 to 600
- key_rows: bfloat16 [6144, 1024], P('ep', 'tp'), may hold values from -6 to 6
- value_rows: bfloat16 [6144, 1024], P('ep', 'tp'), may hold values from -6 to 6
- cum_gate: float32 [16, 6144], P('tp'), may hold values from -615 to 0, as said below
- out_weight: bfloat16 [1024, 2048], P(None, 'tp'), may hold values from -0.1875 to 0.1875
- moe_input: bfloat16 [1536, 2048], P('ep'), may hold values from -6 to 6
- moe_gain: float32 [2048], replicated, may hold values from 0.1 to 1.9
- routes: int32 [1536, 3], P('ep'), may hold values from 0 to 31, all different within a row; in each aligned block of 192 rows (0 to 191, 192 to 383, ...) at most 36 rows name the same one
- route_weight: float32 [1536, 3], P('ep'), may hold values from 0.2 to 1.5
- expert_gate: bfloat16 [32, 2048, 512], P('ep', None, 'tp'), may hold values from -0.125 to 0.125
- expert_up: bfloat16 [32, 2048, 512], P('ep', None, 'tp'), may hold values from -0.125 to 0.125
- expert_down: bfloat16 [32, 512, 2048], P('ep', None, 'tp'), may hold values from -0.25 to 0.25
- shared_gate: bfloat16 [2048, 512], P(None, 'tp'), may hold values from -0.125 to 0.125
- shared_up: bfloat16 [2048, 512], P(None, 'tp'), may hold values from -0.125 to 0.125
- shared_down: bfloat16 [512, 2048], P(None, 'tp'), may hold values from -0.25 to 0.25
Outputs:
- mixer_out: bfloat16 [6144, 2048], P('ep', 'tp')
- moe_out: bfloat16 [1536, 2048], P('ep', 'tp')
Inputs may be any that keep to these rules, and one draw needn't show every extreme that they name: Non-increasing along positions: cum_gate[h, t] is the sum of the log forget gates of head h over positions 0 to t. `routes`: the 3 experts of a token differ. In each aligned block of 192 tokens no expert is named by more than 36 tokens, a bound that some block reaches.
All inputs are finite; a program needn't handle non-finite values.
Results may differ from a plain program's by a relative error of at most 0.0068.
Values may be sent and summed in bfloat16 or wider, within the bound.
A program may use at most 64 MiB of HBM per device.

v0:
```python
import jax
import jax.numpy as jnp
from jax import lax
from jax.sharding import PartitionSpec as P

HEAD = 64


neg_fill = -1e30
norm_eps = 1e-06


def local(
    query_rows,
    key_rows,
    value_rows,
    cum_gate,
    out_weight,
    moe_input,
    moe_gain,
    routes,
    route_weight,
    expert_gate,
    expert_up,
    expert_down,
    shared_gate,
    shared_up,
    shared_down,
):
    row_count = query_rows.shape[0]
    width = query_rows.shape[1]
    local_heads = width // HEAD
    scale = HEAD ** (-0.5)
    first_row = lax.axis_index("ep") * row_count
    last_row = first_row + row_count - 1
    query_heads = query_rows.reshape(row_count, local_heads, HEAD)
    query_gate = lax.dynamic_slice_in_dim(cum_gate, first_row, row_count, 1)
    query_pos = first_row + jnp.arange(row_count, dtype=jnp.int32)
    key_value = jnp.concatenate([key_rows, value_rows], axis=1)
    initial = (
        jnp.full((local_heads, row_count), neg_fill, jnp.float32),
        jnp.zeros((local_heads, row_count), jnp.float32),
        jnp.zeros((local_heads, row_count, HEAD), jnp.float32),
    )
    shard_rows = lax.all_gather(key_value, "ep", axis=0, tiled=True)
    piece_len = shard_rows.shape[0]
    key_span = 512

    def one_span(state_in, span_index):
        span_start = span_index * key_span

        def update(state_old):
            running_max, denominator, weighted = state_old
            block = lax.dynamic_slice_in_dim(shard_rows, span_index * key_span, key_span, 0)
            keys_block = block[:, :width].reshape(key_span, local_heads, HEAD)
            values_block = block[:, width:].reshape(key_span, local_heads, HEAD)
            key_gate = lax.dynamic_slice_in_dim(cum_gate, span_start, key_span, 1)
            scores = (
                jnp.einsum(
                    "qhd,khd->hqk", query_heads, keys_block, preferred_element_type=jnp.float32
                )
                * scale
            )
            scores = scores + query_gate[:, :, None] - key_gate[:, None, :]
            causal = (span_start + jnp.arange(key_span, dtype=jnp.int32))[None, :] <= query_pos[
                :, None
            ]
            scores = jnp.where(causal[None], scores, neg_fill)
            new_max = jnp.maximum(running_max, jnp.max(scores, axis=2))
            expon = jnp.where(causal[None], jnp.exp(scores - new_max[:, :, None]), 0.0)
            rescale = jnp.exp(running_max - new_max)
            denominator = denominator * rescale + jnp.sum(expon, axis=2)
            weighted = weighted * rescale[:, :, None] + jnp.einsum(
                "hqk,khd->hqd",
                expon.astype(jnp.bfloat16),
                values_block,
                preferred_element_type=jnp.float32,
            )
            return (new_max, denominator, weighted)

        state_next = lax.cond(span_start <= last_row, update, lambda unchanged: unchanged, state_in)
        return (state_next, None)

    state_out, _ = lax.scan(one_span, initial, jnp.arange(piece_len // key_span, dtype=jnp.int32))
    running_max, denominator, weighted = state_out
    heads_out = (weighted / denominator[:, :, None]).transpose(1, 0, 2).reshape(row_count, width)
    heads_out = heads_out.astype(jnp.bfloat16)
    token_count = moe_input.shape[0]
    top_count = routes.shape[1]
    local_experts = expert_gate.shape[0]
    ep_count = lax.axis_size("ep")
    expert_count = local_experts * ep_count
    capacity = 2 * token_count * top_count // expert_count
    column_count = expert_down.shape[2]
    first_column = lax.axis_index("tp") * column_count
    moe_rows = moe_input.astype(jnp.float32)
    normed = (
        moe_rows
        * lax.rsqrt(jnp.mean(moe_rows * moe_rows, axis=1, keepdims=True) + norm_eps)
        * moe_gain
    ).astype(jnp.bfloat16)
    flat_routes = routes.reshape(-1)
    one_hot = (flat_routes[:, None] == jnp.arange(expert_count, dtype=jnp.int32)[None, :]).astype(
        jnp.int32
    )
    ranks = jnp.sum(jnp.cumsum(one_hot, axis=0) * one_hot, axis=1) - 1
    slot_index = flat_routes * capacity + ranks
    pair_token = jnp.arange(token_count * top_count, dtype=jnp.int32) // top_count
    slot_token = (
        jnp.full((expert_count * capacity,), token_count, jnp.int32).at[slot_index].set(pair_token)
    )
    padded = jnp.concatenate([normed, jnp.zeros((1, normed.shape[1]), jnp.bfloat16)], axis=0)
    outgoing = lax.dynamic_slice_in_dim(padded, first_column, column_count, 1)[slot_token]
    outgoing = outgoing.reshape(ep_count, local_experts, capacity, outgoing.shape[1])
    arrived = lax.all_to_all(outgoing, "ep", split_axis=0, concat_axis=0, tiled=True)
    arrived = lax.all_gather(arrived, "tp", axis=3, tiled=True)
    gate_val = jnp.einsum(
        "aecd,edf->aecf", arrived, expert_gate, preferred_element_type=jnp.float32
    )
    up_val = jnp.einsum("aecd,edf->aecf", arrived, expert_up, preferred_element_type=jnp.float32)
    hidden = (jax.nn.silu(gate_val) * up_val).astype(jnp.bfloat16)
    hidden = lax.all_gather(hidden, "tp", axis=3, tiled=True)
    result = jnp.einsum(
        "aecf,efd->aecd", hidden, expert_down, preferred_element_type=jnp.float32
    ).astype(jnp.bfloat16)
    returned = lax.all_to_all(result, "ep", split_axis=0, concat_axis=0, tiled=True)
    picked = returned.reshape(expert_count * capacity, column_count)[slot_index]
    picked = picked.astype(jnp.float32).reshape(token_count, top_count, column_count)
    routed = jnp.sum(picked * route_weight[:, :, None], axis=1)
    shared_hidden = (
        jax.nn.silu(jnp.dot(normed, shared_gate, preferred_element_type=jnp.float32))
        * jnp.dot(normed, shared_up, preferred_element_type=jnp.float32)
    ).astype(jnp.bfloat16)
    heads_all, shared_all = (
        lax.all_gather(heads_out, "tp", axis=1, tiled=True),
        lax.all_gather(shared_hidden, "tp", axis=1, tiled=True),
    )
    mixer_sum = jnp.dot(heads_all, out_weight, preferred_element_type=jnp.float32)
    moe_total = routed + jnp.dot(shared_all, shared_down, preferred_element_type=jnp.float32)
    return (mixer_sum.astype(jnp.bfloat16), moe_total.astype(jnp.bfloat16))


def solution(mesh):
    placed = (
        P("ep", "tp"),
        P("ep", "tp"),
        P("ep", "tp"),
        P("tp", None),
        P(None, "tp"),
        P("ep", None),
        P(),
        P("ep", None),
        P("ep", None),
        P("ep", None, "tp"),
        P("ep", None, "tp"),
        P("ep", None, "tp"),
        P(None, "tp"),
        P(None, "tp"),
        P(None, "tp"),
    )
    return jax.shard_map(
        local, mesh=mesh, in_specs=placed, out_specs=(P("ep", "tp"), P("ep", "tp")), check_vma=False
    )
```

profile of v0, /device:TPU:0, one launch (start us, length us, event | category | flops | bytes accessed | tf_op | source)
XLA Modules:
  0.0 447.6 jit_solution(2679872729784148897)
XLA Ops:
  7.2 0.8 broadcast_multiply_fusion
  8.9 1.4 fusion.23
  10.8 1.5 reduce-window.6
  12.8 4.1 scatter_custom_fusion
  16.9 1.4 fusion.25
  18.3 4.7 %gather_fusion = bf16[1152,512]{1,0:T(8,128)(2,1)} fusion(bf16[193,512]{1,0:T(8,128)(2,1)S(1)} %pad_dynamic-slice_fusion, s32[2048]{0:T(1024)S(1)} %pad_clamp_fusion), kind=kCustom, calls=%fused_computation | custom fusion | bytes 2363904 | tf_op jit(solution)/shard_map/gather | solution.py:113
  23.0 2.9 reshape.119
  25.9 1.9 copy.41
  27.9 35.5 %all_to_all.10 = bf16[8,4,36,512]{3,1,2,0:T(4,128)(2,1)S(1)} all-to-all(bf16[8,4,36,512]{3,1,2,0:T(4,128)(2,1)S(1)} %copy.41), channel_id=1, replica_groups=mesh['ep'=8,'tp'=4] {'ep'}, dimensions={0} | all-to-all | bytes 2359296 | tf_op jit(solution)/shard_map/all_to_all | solution.py:115
  63.4 1.4 copy.42
  64.8 60.2 %all-gather.9.cloned.1.call-done = bf16[8,4,36,2048]{3,2,0,1:T(8,128)(2,1)} async-done(((bf16[8,4,36,512]{3,2,0,1:T(8,128)(2,1)}), bf16[8,4,36,2048]{3,2,0,1:T(8,128)(2,1)}) %all-gather.9.cloned.1.call-update) | async-done | bytes 4718608 | tf_op jit(solution)/shard_map/all_gather | solution.py:116
  125.0 4.8 %fusion.29 = f32[8,4,36,128]{3,2,0,1:T(8,128)S(1)} fusion(bf16[8,4,36,2048]{3,2,0,1:T(8,128)(2,1)} %all-gather.9.cloned.1.call-done, bf16[4,2048,128]{2,1,0:T(8,128)(2,1)} %param.28), kind=kOutput, calls=%fused_computation.37 | convolution fusion | flops 603979776 | bytes 7405568 | tf_op jit(solution)/shard_map/aecd,edf->aecf/dot_general | solution.py:117
  130.3 2.3 fusion.38
  132.7 1.2 copy.35
  133.9 1.9 copy.34
  135.8 1.9 pad_maximum_fusion
  137.7 1.9 copy.36
  140.4 21.0 %all-gather.11.cloned.1.call-done = bf16[8,4,36,512]{3,2,0,1:T(8,128)(2,1)} async-done(((bf16[8,4,36,128]{3,2,0,1:T(8,128)(2,1)}), bf16[8,4,36,512]{3,2,0,1:T(8,128)(2,1)}) %all-gather.11.cloned.1.call-update) | async-done | bytes 1179664 | tf_op jit(solution)/shard_map/all_gather | solution.py:122
  161.3 2.2 fusion.26
  163.5 2.0 copy.43
  165.5 4.6 %all-to-all-start.1 = ((bf16[8,4,36,512]{3,1,2,0:T(4,128)(2,1)}), bf16[8,4,36,512]{3,1,2,0:T(4,128)(2,1)}, u32[]{:S(2)}, u32[]{:S(2)}) async-start(bf16[8,4,36,512]{3,1,2,0:T(4,128)(2,1)} %copy.43), calls=%async_computation.1 | async-start | bytes 2359296 | tf_op jit(solution)/shard_map/all_to_all | solution.py:126
  170.3 81.3 %all-gather.5.cloned.1.call-done = bf16[6144,512]{0,1:T(8,128)(2,1)} async-done(((bf16[768,512]{0,1:T(8,128)(2,1)}), bf16[6144,512]{0,1:T(8,128)(2,1)}) %all-gather.5.cloned.1.call-update) | async-done | bytes 6291472 | tf_op jit(solution)/shard_map/all_gather | solution.py:45
  251.6 0.9 broadcast_in_dim.51
  252.6 39.0 %while.15 = (s32[]{:T(128)}, f32[4,768]{1,0:T(4,128)S(1)}, f32[4,768]{1,0:T(4,128)S(1)}, f32[4,768,64]{1,2,0:T(8,128)}, s32[12]{0:T(128)S(1)}, /*index=5*/s32[]{...) while((s32[]{:T(128)}, f32[4,768]{1,0:T(4,128)S(1)}, ...), condition=%wide.region_5.6_spmd.clone, body=%wide.region_0.5_spmd.clone.sunk | while | flops 433331456 | bytes 30568932 | solution.py:84
  253.9 11.5 %conditional.3 = ((f32[4,768]{1,0:T(4,128)S(1)}, f32[4,768]{1,0:T(4,128)S(1)}, f32[4,768,64]{1,2,0:T(8,128)})) conditional(s32[]{:T(128)} %convert_element_type.85, (f32[4,768]{1,0:T(4,128)S(1)}, f32[4,768]{1,0:T(4,128)S(1)}, f32[4,768,64]{1,2,0:T(8,128)}) %tuple.39, (s32[]{:T(128)}, s32[]{:T(128)}, s32[]{:T(128)}, bf16[6144,512]{0,1:T(8,128)(2,1)}, ...), branch_computations={%region_1.1_spmd, %region_2.4_spmd} | conditional | flops 433331456 | bytes 30565576 | solution.py:81
  255.6 1.1 fusion.50
  256.7 2.9 fusion.4
  259.6 2.3 fusion.3
  262.0 2.5 fusion.8
  264.5 0.9 copy-done.3
  266.7 11.5 %conditional.3 = ((f32[4,768]{1,0:T(4,128)S(1)}, f32[4,768]{1,0:T(4,128)S(1)}, f32[4,768,64]{1,2,0:T(8,128)})) conditional(s32[]{:T(128)} %convert_element_type.85, (f32[4,768]{1,0:T(4,128)S(1)}, f32[4,768]{1,0:T(4,128)S(1)}, f32[4,768,64]{1,2,0:T(8,128)}) %tuple.39, (s32[]{:T(128)}, s32[]{:T(128)}, s32[]{:T(128)}, bf16[6144,512]{0,1:T(8,128)(2,1)}, ...), branch_computations={%region_1.1_spmd, %region_2.4_spmd} | conditional | flops 433331456 | bytes 30565576 | solution.py:81
  268.4 1.1 fusion.50
  269.5 2.9 fusion.4
  272.4 2.3 fusion.3
  274.8 2.5 fusion.8
  277.3 0.9 copy-done.3
  291.6 1.9 divide_convert_fusion
  294.4 1.4 fusion.51
  295.8 1.4 fusion.42
  297.2 8.7 %all_gather.19 = bf16[192,512]{1,0:T(8,128)(2,1)S(1)} all-gather(bf16[192,128]{1,0:T(8,128)(2,1)S(1)} %fusion.42), channel_id=1, replica_groups=mesh['ep'=8,'tp'=4] {'tp'}, dimensions={1}, use_global_device_ids=true | all-gather | bytes 245760 | tf_op jit(solution)/shard_map/all_gather | solution.py:136
  305.9 2.6 copy.44
  308.5 2.1 reshape.120
  310.7 3.3 gather_fusion.1
  313.9 2.5 reshape.122
  316.4 2.4 multiply_reduce_fusion
  318.9 1.0 fusion.41
  319.8 117.7 %all-gather.7.cloned.1.call-done = bf16[768,1024]{0,1:T(8,128)(2,1)} async-done(((bf16[768,256]{0,1:T(8,128)(2,1)}), bf16[768,1024]{0,1:T(8,128)(2,1)}) %all-gather.7.cloned.1.call-update) | async-done | bytes 1572880 | tf_op jit(solution)/shard_map/all_gather | solution.py:135
  437.5 3.6 convolution_convert_fusion
  (98 shorter events, 14.4 us)
Async XLA Ops:
  7.2 154.2 %copy-start = (bf16[4,512,512]{2,1,0:T(8,128)(2,1)S(1)}, bf16[4,512,512]{2,1,0:T(8,128)(2,1)}, u32[]{:S(2)}) copy-start(bf16[4,512,512]{2,1,0:T(8,128)(2,1)} %param.30) | copy-start | bytes 6291460
  7.2 117.9 %all-gather.9.cloned.1.call-start = ((), (), s32[]{:S(2)}) async-start(), calls=%async_computation.4 | async-start | bytes 6553600 | tf_op jit(solution)/shard_map/all_gather | solution.py:116
  64.8 96.6 %all-gather.11.cloned.1.call-start = ((), (), s32[]{:S(2)}) async-start(), calls=%async_computation.5 | async-start | bytes 1638400 | tf_op jit(solution)/shard_map/all_gather | solution.py:122
  125.0 4.8 %copy-start.1 = (bf16[8,4,36,2048]{3,2,0,1:T(8,128)(2,1)S(1)}, bf16[8,4,36,2048]{3,2,0,1:T(8,128)(2,1)}, u32[]{:S(2)}) copy-start(bf16[8,4,36,2048]{3,2,0,1:T(8,128)(2,1)} %all-gather.9.cloned.1.call-done) | copy-start | bytes 14155780
  125.0 5.3 %copy-start.7 = (bf16[4,2048,128]{2,1,0:T(8,128)(2,1)S(1)}, bf16[4,2048,128]{2,1,0:T(8,128)(2,1)}, u32[]{:S(2)}) copy-start(bf16[4,2048,128]{2,1,0:T(8,128)(2,1)} %param.29) | copy-start | bytes 6291460
  132.6 119.0 %all-gather.5.cloned.1.call-start = ((), (), s32[]{:S(2)}) async-start(), calls=%async_computation.2 | async-start | bytes 7077888 | tf_op jit(solution)/shard_map/all_gather | solution.py:45
  165.5 140.4 %all-to-all-start.1 = ((bf16[8,4,36,512]{3,1,2,0:T(4,128)(2,1)}), bf16[8,4,36,512]{3,1,2,0:T(4,128)(2,1)}, u32[]{:S(2)}, u32[]{:S(2)}) async-start(bf16[8,4,36,512]{3,1,2,0:T(4,128)(2,1)} %copy.43), calls=%async_computation.1 | async-start | bytes 2359296 | tf_op jit(solution)/shard_map/all_to_all | solution.py:126
  170.1 267.4 %all-gather.7.cloned.1.call-start = ((), (), s32[]{:S(2)}) async-start(), calls=%async_computation.3 | async-start | bytes 1966080 | tf_op jit(solution)/shard_map/all_gather | solution.py:135
  252.6 41.0 %copy-start.6 = (f32[192,3]{0,1:T(4,128)S(1)}, f32[192,3]{0,1:T(4,128)}, u32[]{:S(2)}) copy-start(f32[192,3]{0,1:T(4,128)} %param.27) | copy-start | bytes 6916
  259.6 2.4 copy-start.2
  264.5 0.9 copy-start.3
  272.4 2.4 copy-start.2
  277.3 0.9 copy-start.3
  313.9 2.5 copy-start.5
  313.9 5.0 %copy-start.4 = (bf16[512,512]{1,0:T(8,128)(2,1)S(1)}, bf16[512,512]{1,0:T(8,128)(2,1)}, u32[]{:S(2)}) copy-start(bf16[512,512]{1,0:T(8,128)(2,1)} %param.33) | copy-start | bytes 1572868
Sparse Core Ops, SparseCore 0:
  64.9 60.0 all-gather.8
  132.8 28.5 all-gather.10
  163.5 88.0 all-gather.4
  293.7 143.7 all-gather.6
where the time goes:
time: 450 us; the launch traced here: 448 us
  waiting for transfers between devices  280 us (62%)
  local copies, waits for them, and re-layouts  50.3 us (11%)
  blocking collectives  44.2 us (10%)
  matrix products  27.4 us (6%)
  other arithmetic  16.8 us (4%)
  between operations  14 us (3%)
  loops' own time  9.67 us (2%)
  starting transfers between devices  4.94 us (1%)
    all_gather x1, waiting for transfers between devices, local(): lax.all_gather(heads_out, 'tp', axis=1, tiled=True)  118 us
    all_gather x1, waiting for transfers between devices, local(): shard_rows = lax.all_gather(key_value, 'ep', axis=0, tiled=True)  81.3 us
    all_gather x1, waiting for transfers between devices, local(): arrived = lax.all_gather(arrived, 'tp', axis=3, tiled=True)  60.2 us
    all_to_all x1, blocking collectives, local(): lax.all_to_all(outgoing, 'ep', split_axis=0, concat_axis=0, tiled=True)  35.5 us
    all_gather x1, waiting for transfers between devices, local(): hidden = lax.all_gather(hidden, 'tp', axis=3, tiled=True)  21 us
  transfers between devices with their start and end apart: 5, of which 4 were waited for; matrix products, arithmetic and copies ran while one was open for 13% of the time, Pallas kernels for 0%

commit v1 on v0

v1 whole, which is shorter than its diff:
```python
import functools

import jax
import jax.numpy as jnp
from jax import lax
from jax.experimental import pallas as pl
from jax.experimental.pallas import tpu as pltpu
from jax.sharding import PartitionSpec as P

HEAD = 64
LANES = 128
CORES = 2

neg_fill = -1e30
norm_eps = 1e-06


def attention_kernel(
    heads,
    q_ref,
    kv_ref,
    gate_ref,
    out_ref,
    held,
    acc,
    row_max,
    up_send,
    side_send,
    recv_sem,
):
    rows = kv_ref.shape[0]
    width = kv_ref.shape[1] // 2
    pairs = width // LANES
    tile = 256 if rows % 256 == 0 else rows
    tiles = rows // tile
    me = lax.axis_index("ep")
    chips = lax.axis_size("ep") // CORES
    chip = me // CORES
    core = me % CORES
    other = 1 - core

    barrier = pltpu.get_barrier_semaphore()

    def greet(index):
        pl.semaphore_signal(barrier, inc=1, device_id={"ep": index})

    greet(chip * CORES + other)

    @pl.when(chip > 0)
    def _():
        greet(me - CORES)

    @pl.when(chip < chips - 1)
    def _():
        greet(me + CORES)

    neighbours = 1 + jnp.where(chip > 0, 1, 0) + jnp.where(chip < chips - 1, 1, 0)
    pl.semaphore_wait(barrier, neighbours)

    def up_copy(src, slot):
        return pltpu.make_async_remote_copy(
            src_ref=src,
            dst_ref=held.at[slot],
            send_sem=up_send.at[slot],
            recv_sem=recv_sem.at[slot],
            device_id={"ep": me + CORES},
        )

    def side_copy(src, slot):
        return pltpu.make_async_remote_copy(
            src_ref=src,
            dst_ref=held.at[slot],
            send_sem=side_send.at[slot],
            recv_sem=recv_sem.at[slot],
            device_id={"ep": chip * CORES + other},
        )

    @pl.when(chip < chips - 1)
    def _():
        up_copy(kv_ref, me).start()

    @pl.when(core == 0)
    def _():
        side_copy(kv_ref, me).start()

    ones = jnp.ones((rows, LANES), jnp.bfloat16)

    def block_step(block, source, first):
        for pair in range(pairs):
            lanes = pl.ds(pair * LANES, LANES)
            value_lanes = pl.ds(width + pair * LANES, LANES)

            def one_tile(index, carry):
                start = pl.multiple_of(index * tile, tile)
                q_rows = pl.ds(start, tile)
                gates = gate_ref[pl.ds(pl.multiple_of(block * rows, rows), rows), lanes]
                keys = jnp.concatenate([source[:, lanes], gates], axis=1)
                values = jnp.concatenate([source[:, value_lanes], ones], axis=1)
                for head in range(2 * pair, min(2 * pair + 2, heads)):
                    scores = lax.dot_general(
                        q_ref[head, q_rows, :],
                        keys,
                        (((1,), (1,)), ((), ())),
                        preferred_element_type=jnp.float32,
                    )
                    if first:
                        q_pos = start + lax.broadcasted_iota(jnp.int32, scores.shape, 0)
                        k_pos = lax.broadcasted_iota(jnp.int32, scores.shape, 1)
                        scores = jnp.where(k_pos <= q_pos, scores, neg_fill)
                        top = jnp.max(scores, axis=1, keepdims=True)
                        new_max = jnp.broadcast_to(top, (tile, LANES))
                    else:
                        old_max = row_max[head, q_rows, :]
                        new_max = jnp.maximum(old_max, jnp.max(scores, axis=1, keepdims=True))
                    probs = jnp.exp(scores - new_max[:, :1]).astype(jnp.bfloat16)
                    add = jnp.dot(probs, values, preferred_element_type=jnp.float32)
                    if not first:
                        keep = jnp.exp(old_max - new_max)
                        add = add + acc[head, q_rows, :] * jnp.concatenate([keep, keep], axis=1)
                    acc[head, q_rows, :] = add
                    row_max[head, q_rows, :] = new_max
                return carry

            lax.fori_loop(0, tiles, one_tile, 0)

    block_step(me, kv_ref, True)

    def remote_step(step, carry):
        turn = step - core + 2
        own_core = turn % 2 == 0
        slot = (chip - turn // 2) * CORES + jnp.where(own_core, core, other)
        landed = held.at[slot]
        side_copy(landed, slot).wait_recv()

        @pl.when(jnp.logical_and(own_core, chip < chips - 1))
        def _():
            up_copy(landed, slot).start()

        @pl.when(own_core)
        def _():
            side_copy(landed, slot).start()

        block_step(slot, landed, False)
        return carry

    lax.fori_loop(0, me, remote_step, 0)

    for head in range(heads):
        pair, part = head // 2, head % 2
        spot = slice(part * HEAD, part * HEAD + HEAD)
        whole = acc[head, :, :LANES] / acc[head, :, LANES:]
        out_ref[:, head * HEAD : (head + 1) * HEAD] = whole[:, spot].astype(out_ref.dtype)

    def finish(step, carry):
        slot = (chip - step) * CORES + core

        @pl.when(chip < chips - 1)
        def _():
            up_copy(held.at[slot], slot).wait_send()

        @pl.when(step > 0)
        def _():
            side_copy(held.at[slot], slot).wait_send()

        return carry

    lax.fori_loop(0, chip + 1, finish, 0)

    @pl.when(core == 0)
    def _():
        side_copy(kv_ref, me).wait_send()


def attention(query_rows, key_rows, value_rows, cum_gate):
    rows, width = query_rows.shape
    heads = width // HEAD
    pairs = (heads + 1) // 2
    ep_count = lax.axis_size("ep")
    padded = pairs * LANES
    if padded > width:
        spare = ((0, 0), (0, padded - width))
        query_rows, key_rows, value_rows = (
            jnp.pad(a, spare) for a in (query_rows, key_rows, value_rows)
        )
    key_value = jnp.concatenate([key_rows, value_rows], axis=1)
    scaled = query_rows * jnp.asarray(HEAD**-0.5, jnp.bfloat16)
    lane = jnp.arange(LANES)
    parts = []
    for head in range(heads):
        pair, part = head // 2, head % 2
        piece = scaled[:, pair * LANES : (pair + 1) * LANES]
        piece = jnp.where((lane // HEAD == part)[None], piece, 0)
        marks = ((lane // 3) == part).astype(jnp.bfloat16)
        parts.append(jnp.concatenate([piece, jnp.broadcast_to(marks, (rows, LANES))], axis=1))
    queries = jnp.stack(parts)
    minus = -cum_gate
    high = lax.reduce_precision(minus, 8, 7)
    rest = minus - high
    mid = lax.reduce_precision(rest, 8, 7)
    low = rest - mid
    terms = jnp.stack([high, mid, low], axis=1).astype(jnp.bfloat16)
    if heads % 2:
        terms = jnp.concatenate([terms, jnp.zeros_like(terms[:1])], axis=0)
    terms = terms.reshape(pairs, 6, cum_gate.shape[1])
    terms = jnp.pad(terms, ((0, 0), (0, LANES - 6), (0, 0)))
    gates = terms.reshape(pairs * LANES, cum_gate.shape[1]).T
    blocks = ep_count * rows * rows * heads
    return pl.pallas_call(
        functools.partial(attention_kernel, heads),
        out_shape=jax.ShapeDtypeStruct((rows, heads * HEAD), jnp.bfloat16),
        in_specs=[pl.BlockSpec(memory_space=pltpu.VMEM)] * 3,
        out_specs=pl.BlockSpec(memory_space=pltpu.VMEM),
        scratch_shapes=[
            pltpu.VMEM((ep_count, rows, 2 * padded), jnp.bfloat16),
            pltpu.VMEM((heads, rows, 2 * LANES), jnp.float32),
            pltpu.VMEM((heads, rows, LANES), jnp.float32),
            pltpu.SemaphoreType.DMA((ep_count,)),
            pltpu.SemaphoreType.DMA((ep_count,)),
            pltpu.SemaphoreType.DMA((ep_count,)),
        ],
        compiler_params=pltpu.CompilerParams(
            collective_id=0, has_side_effects=True, vmem_limit_bytes=48 * 1024 * 1024
        ),
        cost_estimate=pl.CostEstimate(
            flops=blocks * 2 * 512, bytes_accessed=8 * 1024 * 1024, transcendentals=blocks
        ),
        name="attend",
    )(queries, key_value, gates)


def local(
    query_rows,
    key_rows,
    value_rows,
    cum_gate,
    out_weight,
    moe_input,
    moe_gain,
    routes,
    route_weight,
    expert_gate,
    expert_up,
    expert_down,
    shared_gate,
    shared_up,
    shared_down,
):
    heads_out = attention(query_rows, key_rows, value_rows, cum_gate)
    token_count = moe_input.shape[0]
    top_count = routes.shape[1]
    local_experts = expert_gate.shape[0]
    ep_count = lax.axis_size("ep")
    expert_count = local_experts * ep_count
    capacity = 2 * token_count * top_count // expert_count
    column_count = expert_down.shape[2]
    first_column = lax.axis_index("tp") * column_count
    moe_rows = moe_input.astype(jnp.float32)
    normed = (
        moe_rows
        * lax.rsqrt(jnp.mean(moe_rows * moe_rows, axis=1, keepdims=True) + norm_eps)
        * moe_gain
    ).astype(jnp.bfloat16)
    expert_ids = jnp.arange(expert_count, dtype=jnp.int32)
    chosen = routes[:, :, None] == expert_ids[None, None, :]
    named = jnp.any(chosen, axis=1)
    weight_of = jnp.sum(jnp.where(chosen, route_weight[:, :, None], 0.0), axis=1)
    order = jnp.arange(token_count)
    earlier = (order[None, :] < order[:, None]).astype(jnp.bfloat16)
    ranks = jnp.dot(earlier, named.astype(jnp.bfloat16), preferred_element_type=jnp.float32)
    ranks = jnp.where(named, ranks.astype(jnp.int32), -1)
    slots = jnp.arange(capacity, dtype=jnp.int32)
    place = ranks[:, :, None] == slots[None, None, :]
    pick = place.astype(jnp.bfloat16).reshape(token_count, expert_count * capacity)
    own_columns = lax.dynamic_slice_in_dim(normed, first_column, column_count, 1)
    outgoing = lax.dot_general(
        pick, own_columns, (((0,), (0,)), ((), ())), preferred_element_type=jnp.float32
    ).astype(jnp.bfloat16)
    outgoing = outgoing.reshape(ep_count, local_experts, capacity, column_count)
    arrived = lax.all_to_all(outgoing, "ep", split_axis=0, concat_axis=0, tiled=True)
    arrived = lax.all_gather(arrived, "tp", axis=3, tiled=True)
    gate_val = jnp.einsum(
        "aecd,edf->aecf", arrived, expert_gate, preferred_element_type=jnp.float32
    )
    up_val = jnp.einsum("aecd,edf->aecf", arrived, expert_up, preferred_element_type=jnp.float32)
    hidden = (jax.nn.silu(gate_val) * up_val).astype(jnp.bfloat16)
    hidden = lax.all_gather(hidden, "tp", axis=3, tiled=True)
    result = jnp.einsum(
        "aecf,efd->aecd", hidden, expert_down, preferred_element_type=jnp.float32
    ).astype(jnp.bfloat16)
    returned = lax.all_to_all(result, "ep", split_axis=0, concat_axis=0, tiled=True)
    returned = returned.reshape(expert_count * capacity, column_count)
    weight_high = lax.reduce_precision(weight_of, 8, 7)
    weight_low = weight_of - weight_high
    routed = 0.0
    for weight in (weight_high, weight_low):
        spread = jnp.where(place, weight[:, :, None], 0.0).astype(jnp.bfloat16)
        routed = routed + jnp.dot(
            spread.reshape(token_count, expert_count * capacity),
            returned,
            preferred_element_type=jnp.float32,
        )
    shared_hidden = (
        jax.nn.silu(jnp.dot(normed, shared_gate, preferred_element_type=jnp.float32))
        * jnp.dot(normed, shared_up, preferred_element_type=jnp.float32)
    ).astype(jnp.bfloat16)
    heads_all, shared_all = (
        lax.all_gather(heads_out, "tp", axis=1, tiled=True),
        lax.all_gather(shared_hidden, "tp", axis=1, tiled=True),
    )
    mixer_sum = jnp.dot(heads_all, out_weight, preferred_element_type=jnp.float32)
    moe_total = routed + jnp.dot(shared_all, shared_down, preferred_element_type=jnp.float32)
    return (mixer_sum.astype(jnp.bfloat16), moe_total.astype(jnp.bfloat16))


def solution(mesh):
    placed = (
        P("ep", "tp"),
        P("ep", "tp"),
        P("ep", "tp"),
        P("tp", None),
        P(None, "tp"),
        P("ep", None),
        P(),
        P("ep", None),
        P("ep", None),
        P("ep", None, "tp"),
        P("ep", None, "tp"),
        P("ep", None, "tp"),
        P(None, "tp"),
        P(None, "tp"),
        P(None, "tp"),
    )
    return jax.shard_map(
        local, mesh=mesh, in_specs=placed, out_specs=(P("ep", "tp"), P("ep", "tp")), check_vma=False
    )
```

time: 450 us -> 246 us (0.55)
  waiting for transfers between devices: 280 us -> 62.1 us
  starting transfers between devices: 4.94 us -> 47.4 us
  local copies, waits for them, and re-layouts: 50.3 us -> 27.6 us
  Pallas kernels: 0 us -> 19.1 us
  loops' own time: 9.67 us -> 0 us
  other arithmetic: 16.8 us -> 8.29 us
  matrix products: 27.4 us -> 20.8 us
    all_gather x1, waiting for transfers between devices: 118 us -> 3.82 us  [local(): lax.all_gather(heads_out, 'tp', axis=1, tiled=True)]
    all_gather x1 -> x0, waiting for transfers between devices: 81.3 us -> none  [local(): shard_rows = lax.all_gather(key_value, 'ep', axis=0, tiled=True)]
    all_to_all x1, starting transfers between devices: 4.6 us -> 47.3 us  [local(): lax.all_to_all(result, 'ep', split_axis=0, concat_axis=0, tiled=True)]
    pallas_call x0 -> x1, Pallas kernels: none -> 19.1 us  [attention(): pl.pallas_call(functools.partial(attention_kernel, heads), out_shape=jax....]
    all_gather x1, waiting for transfers between devices: 21 us -> 6.23 us  [local(): hidden = lax.all_gather(hidden, 'tp', axis=3, tiled=True)]
    all_gather x1, waiting for transfers between devices: 60.2 us -> 49.9 us  [local(): arrived = lax.all_gather(arrived, 'tp', axis=3, tiled=True)]
    dynamic_slice x16 -> x0, local copies, waits for them, and re-layouts: 10.1 us -> none  [the longest x12 7.79 us: local(): lax.scan(one_span, initial, jnp.arange(piece_len // key_span, dtype=jnp.i...]
    another operation x13 -> x0, loops' own time: 9.67 us -> none  [the longest x1 8.06 us: local(): lax.scan(one_span, initial, jnp.arange(piece_len // key_span, dtype=jnp.i...]
  transfers between devices with their start and end apart: 5 -> 4, of which waited for: 4 -> 4; matrix products, arithmetic and copies ran while one was open for 13% -> 11% of each run, Pallas kernels for 0% -> 8%
where the time goes in v1:
time: 246 us
  waiting for transfers between devices  62.1 us (25%)
  starting transfers between devices  47.4 us (19%)
  blocking collectives  46.3 us (19%)
  local copies, waits for them, and re-layouts  27.6 us (11%)
  matrix products  20.8 us (8%)
  Pallas kernels  19.1 us (8%)
  between operations  14.1 us (6%)
  other arithmetic  8.29 us (3%)
    all_gather x1, waiting for transfers between devices, local(): arrived = lax.all_gather(arrived, 'tp', axis=3, tiled=True)  49.9 us
    all_to_all x1, starting transfers between devices, local(): lax.all_to_all(result, 'ep', split_axis=0, concat_axis=0, tiled=True)  47.3 us
    all_to_all x1, blocking collectives, local(): lax.all_to_all(outgoing, 'ep', split_axis=0, concat_axis=0, tiled=True)  35.5 us
    pallas_call x1, Pallas kernels, attention(): pl.pallas_call(functools.partial(attention_kernel, heads), out_shape=jax....  19.1 us
    all_gather x1, blocking collectives, local(): lax.all_gather(shared_hidden, 'tp', axis=1, tiled=True)  10.7 us
    all_gather x1, waiting for transfers between devices, local(): hidden = lax.all_gather(hidden, 'tp', axis=3, tiled=True)  6.23 us
    unnamed x30, local copies, waits for them, and re-layouts  5.25 us
  transfers between devices with their start and end apart: 4, of which 4 were waited for; matrix products, arithmetic and copies ran while one was open for 11% of the time, Pallas kernels for 8%

profile of v1, /device:TPU:0, one launch (start us, length us, event | category | flops | bytes accessed | tf_op | source)
XLA Modules:
  0.0 245.6 jit_solution(226767488982848728)
XLA Ops:
  7.2 1.5 fusion.9
  8.7 0.7 fusion.34
  9.5 0.2 fusion.30
  9.6 0.1 eq.92
  9.7 1.2 eq.95
  10.9 0.1 eq.97
  11.0 1.5 fusion.11
  12.5 0.9 copy-done.5
  13.4 1.6 convolution_convert_fusion
  14.9 2.1 reshape.129
  17.0 0.6 copy.37
  17.7 35.5 %all_to_all.10 = bf16[8,4,36,512]{3,1,2,0:T(4,128)(2,1)S(1)} all-to-all(bf16[8,4,36,512]{3,1,2,0:T(4,128)(2,1)S(1)} %copy.37), channel_id=1, replica_groups=mesh['ep'=8,'tp'=4] {'ep'}, dimensions={0} | all-to-all | bytes 2359296 | tf_op jit(solution)/shard_map/all_to_all | solution.py:279
  53.2 1.4 copy.38
  54.8 0.1 pad_maximum_fusion.2
  54.9 0.1 copy.35
  55.0 0.1 convert_element_type.85
  55.1 2.1 pad.4
  57.2 4.9 %copy.44 = bf16[256,6144]{0,1:T(8,128)(2,1)} copy(bf16[256,6144]{1,0:T(8,128)(2,1)} %bitcast.76) | data formatting | bytes 6291456 | tf_op jit(solution)/shard_map/reshape | solution.py:206
  62.1 1.1 pad_maximum_fusion.1.kv_ref
  63.3 0.1 broadcast_select_fusion.3
  63.3 0.2 maximum_bitcast_fusion
  63.6 1.4 pad_maximum_fusion.q_ref
  65.0 49.9 %all-gather.6.cloned.1.call-done = bf16[8,4,36,2048]{3,2,0,1:T(8,128)(2,1)} async-done(((bf16[8,4,36,512]{3,2,0,1:T(8,128)(2,1)}), bf16[8,4,36,2048]{3,2,0,1:T(8,128)(2,1)}) %all-gather.6.cloned.1.call-update) | async-done | bytes 4718608 | tf_op jit(solution)/shard_map/all_gather | solution.py:280
  114.8 4.8 %fusion.15 = f32[8,4,36,128]{3,2,0,1:T(8,128)S(1)} fusion(bf16[8,4,36,2048]{3,2,0,1:T(8,128)(2,1)} %all-gather.6.cloned.1.call-done, bf16[4,2048,128]{2,1,0:T(8,128)(2,1)} %param.24), kind=kOutput, calls=%fused_computation.19 | convolution fusion | flops 603979776 | bytes 7405568 | tf_op jit(solution)/shard_map/aecd,edf->aecf/dot_general | solution.py:281
  119.7 0.5 copy-done.14
  120.1 2.3 fusion.24
  122.5 1.9 copy-done.1
  124.4 1.4 copy-done.2
  125.8 19.1 %attend.1 = bf16[768,256]{1,0:T(8,128)(2,1)} custom-call(bf16[4,768,256]{2,1,0:T(8,128)(2,1)S(1)} %copy-done.2, bf16[768,512]{1,0:T(8,128)(2,1)S(1)} %pad_maximum_fusion.1.kv_ref, bf16[6144,256]{1,0:T(8,128)(2,1)S(1)} %bitcast.75), custom_call_target="tpu_custom_call" | custom-call | flops 19327352832 | bytes 8388608 | tf_op jit(solution)/shard_map/attend/pallas_call | solution.py:208
  144.9 6.2 %all-gather.8.cloned.1.call-done = bf16[8,4,36,512]{3,2,0,1:T(8,128)(2,1)} async-done(((bf16[8,4,36,128]{3,2,0,1:T(8,128)(2,1)}), bf16[8,4,36,512]{3,2,0,1:T(8,128)(2,1)}) %all-gather.8.cloned.1.call-update) | async-done | bytes 1179664 | tf_op jit(solution)/shard_map/all_gather | solution.py:286
  151.1 2.2 fusion.12
  153.3 1.9 copy.39
  155.2 47.3 %all-to-all-start.1 = ((bf16[8,4,36,512]{3,1,2,0:T(4,128)(2,1)}), bf16[8,4,36,512]{3,1,2,0:T(4,128)(2,1)S(1)}, u32[]{:S(2)}, u32[]{:S(2)}) async-start(bf16[8,4,36,512]{3,1,2,0:T(4,128)(2,1)} %copy.39), calls=%async_computation.1 | async-start | bytes 2359296 | tf_op jit(solution)/shard_map/all_to_all | solution.py:290
  202.6 1.5 select_convert_fusion
  204.2 2.1 convert_element_type.89
  206.3 2.1 convert_element_type.97
  208.4 1.6 fusion.40
  210.0 1.6 fusion.29
  211.7 10.7 %all_gather.15 = bf16[192,512]{1,0:T(8,128)(2,1)S(1)} all-gather(bf16[192,128]{1,0:T(8,128)(2,1)S(1)} %fusion.29), channel_id=1, replica_groups=mesh['ep'=8,'tp'=4] {'tp'}, dimensions={1}, use_global_device_ids=true | all-gather | bytes 245760 | tf_op jit(solution)/shard_map/all_gather | solution.py:308
  222.4 3.8 %all-gather.4.cloned.1.call-done = bf16[768,1024]{1,0:T(8,128)(2,1)} async-done(((bf16[768,256]{1,0:T(8,128)(2,1)}), bf16[768,1024]{1,0:T(8,128)(2,1)}) %all-gather.4.cloned.1.call-update) | async-done | bytes 1572880 | tf_op jit(solution)/shard_map/all_gather | solution.py:307
  226.2 3.6 %convolution_convert_fusion.1 = bf16[768,512]{1,0:T(8,128)(2,1)} fusion(bf16[768,1024]{1,0:T(8,128)(2,1)} %all-gather.4.cloned.1.call-done, bf16[1024,512]{1,0:T(8,128)(2,1)} %param.19), kind=kOutput, calls=%fused_computation.15 | convolution fusion | flops 805699584 | bytes 3407872 | tf_op jit(solution)/shard_map/dot_general | solution.py:310
  229.8 2.2 all-to-all-done.1
  231.9 1.3 copy.40
  233.3 2.1 reshape.130
  235.4 1.6 fusion.39
  237.0 0.5 convolution_add_fusion.1
  237.5 0.6 copy-done.7
  238.1 1.0 fusion.28
  (43 shorter events, 0.4 us)
Async XLA Ops:
  7.2 144.0 %copy-start = (bf16[4,512,512]{2,1,0:T(8,128)(2,1)S(1)}, bf16[4,512,512]{2,1,0:T(8,128)(2,1)}, u32[]{:S(2)}) copy-start(bf16[4,512,512]{2,1,0:T(8,128)(2,1)} %param.26) | copy-start | bytes 6291460
  7.2 107.7 %all-gather.6.cloned.1.call-start = ((), (), s32[]{:S(2)}) async-start(), calls=%async_computation.3 | async-start | bytes 6553600 | tf_op jit(solution)/shard_map/all_gather | solution.py:280
  9.7 1.3 copy-start.12
  10.9 2.5 %copy-start.4 = (s32[192,1152]{0,1:T(8,128)S(1)}, s32[192,1152]{0,1:T(8,128)}, u32[]{:S(2)}) copy-start(s32[192,1152]{0,1:T(8,128)} %eq.95) | copy-start | bytes 2654212
  12.5 0.9 copy-start.5
  53.2 1.5 copy-start.10
  54.6 96.6 %all-gather.8.cloned.1.call-start = ((), (), s32[]{:S(2)}) async-start(), calls=%async_computation.4 | async-start | bytes 1638400 | tf_op jit(solution)/shard_map/all_gather | solution.py:286
  57.2 4.9 %copy-start.9 = (bf16[768,256]{1,0:T(8,128)(2,1)S(1)}, bf16[768,256]{1,0:T(8,128)(2,1)}, u32[]{:S(2)}) copy-start(bf16[768,256]{1,0:T(8,128)(2,1)} %param.17) | copy-start | bytes 1179652
  62.1 1.2 copy-start.8
  114.8 4.8 %copy-start.3 = (bf16[8,4,36,2048]{3,2,0,1:T(8,128)(2,1)S(1)}, bf16[8,4,36,2048]{3,2,0,1:T(8,128)(2,1)}, u32[]{:S(2)}) copy-start(bf16[8,4,36,2048]{3,2,0,1:T(8,128)(2,1)} %all-gather.6.cloned.1.call-done) | copy-start | bytes 14155780
  114.8 5.3 %copy-start.14 = (bf16[4,2048,128]{2,1,0:T(8,128)(2,1)S(1)}, bf16[4,2048,128]{2,1,0:T(8,128)(2,1)}, u32[]{:S(2)}) copy-start(bf16[4,2048,128]{2,1,0:T(8,128)(2,1)} %param.25) | copy-start | bytes 6291460
  122.4 103.8 %all-gather.4.cloned.1.call-start = ((), (), s32[]{:S(2)}) async-start(), calls=%async_computation.2 | async-start | bytes 1966080 | tf_op jit(solution)/shard_map/all_gather | solution.py:307
  122.5 1.9 copy-start.1
  124.4 1.4 copy-start.2
  155.2 47.3 %copy-start.11 = (s32[192,3]{0,1:T(4,128)S(1)}, s32[192,3]{0,1:T(4,128)}, u32[]{:S(2)}) copy-start(s32[192,3]{0,1:T(4,128)} %param.22) | copy-start | bytes 6916
  155.2 47.3 %copy-start.13 = (f32[192,3]{0,1:T(4,128)S(1)}, f32[192,3]{0,1:T(4,128)}, u32[]{:S(2)}) copy-start(f32[192,3]{0,1:T(4,128)} %param.23) | copy-start | bytes 6916
  155.2 76.7 %all-to-all-start.1 = ((bf16[8,4,36,512]{3,1,2,0:T(4,128)(2,1)}), bf16[8,4,36,512]{3,1,2,0:T(4,128)(2,1)S(1)}, u32[]{:S(2)}, u32[]{:S(2)}) async-start(bf16[8,4,36,512]{3,1,2,0:T(4,128)(2,1)} %copy.39), calls=%async_computation.1 | async-start | bytes 2359296 | tf_op jit(solution)/shard_map/all_to_all | solution.py:290
  235.4 1.6 copy-start.6
  237.0 1.0 copy-start.7
Sparse Core Ops, SparseCore 0:
  54.7 60.0 all-gather.5
  122.6 28.5 all-gather.7
  153.0 73.2 all-gather.3

commit v2 on v1

--- a/solution.py
+++ b/solution.py
@@ -20,13 +20,21 @@
     q_ref,
     kv_ref,
     gate_ref,
+    normed_ref,
     out_ref,
+    tokens,
     held,
     acc,
     row_max,
     up_send,
     side_send,
     recv_sem,
+    chip_send,
+    plane_send,
+    piece_recv,
+    block_send,
+    block_recv,
+    own_sem,
 ):
     rows = kv_ref.shape[0]
     width = kv_ref.shape[1] // 2
@@ -41,21 +49,30 @@
 
     barrier = pltpu.get_barrier_semaphore()
 
-    def greet(index):
-        pl.semaphore_signal(barrier, inc=1, device_id={"ep": index})
-
-    greet(chip * CORES + other)
-
-    @pl.when(chip > 0)
-    def _():
-        greet(me - CORES)
-
-    @pl.when(chip < chips - 1)
-    def _():
-        greet(me + CORES)
-
-    neighbours = 1 + jnp.where(chip > 0, 1, 0) + jnp.where(chip < chips - 1, 1, 0)
-    pl.semaphore_wait(barrier, neighbours)
+    def loop(count, body):
+        def step(index, carry):
+            body(index)
+            return carry
+
+        lax.fori_loop(0, count, step, 0)
+
+    def greet(**where):
+        pl.semaphore_signal(barrier, inc=1, device_id=where)
+
+    tp_count = lax.axis_size("tp")
+    tp_me = lax.axis_index("tp")
+    columns = normed_ref.shape[1] // tp_count
+
+    def chip_at(turn):
+        return lax.rem(chip + turn + 1, chips)
+
+    def tp_at(turn):
+        return lax.rem(tp_me + turn + 1, tp_count)
+
+    greet(ep=chip * CORES + other)
+    loop(chips - 1, lambda turn: greet(ep=chip_at(turn) * CORES + core))
+    loop(tp_count - 1, lambda turn: greet(tp=tp_at(turn)))
+    pl.semaphore_wait(barrier, chips + tp_count - 1)
 
     def up_copy(src, slot):
         return pltpu.make_async_remote_copy(
@@ -66,6 +83,15 @@
             device_id={"ep": me + CORES},
         )
 
+    def far_copy(target):
+        return pltpu.make_async_remote_copy(
+            src_ref=kv_ref,
+            dst_ref=held.at[me],
+            send_sem=up_send.at[target * CORES + core],
+            recv_sem=recv_sem.at[me],
+            device_id={"ep": target * CORES + core},
+        )
+
     def side_copy(src, slot):
         return pltpu.make_async_remote_copy(
             src_ref=src,
@@ -75,13 +101,64 @@
             device_id={"ep": chip * CORES + other},
         )
 
+    def lanes_of(index):
+        return pl.ds(pl.multiple_of(index * columns, columns), columns)
+
+    def chip_copy(target):
+        return pltpu.make_async_remote_copy(
+            src_ref=normed_ref.at[:, lanes_of(tp_me)],
+            dst_ref=tokens.at[me, :, lanes_of(tp_me)],
+            send_sem=chip_send.at[target],
+            recv_sem=piece_recv.at[me, tp_me],
+            device_id={"ep": target * CORES + core},
+        )
+
+    def plane_copy(slot, piece, target):
+        place = tokens.at[slot, :, lanes_of(piece)]
+        return pltpu.make_async_remote_copy(
+            src_ref=place,
+            dst_ref=place,
+            send_sem=plane_send.at[slot, target],
+            recv_sem=piece_recv.at[slot, piece],
+            device_id={"tp": target},
+        )
+
+    def block_copy(src, slot):
+        return pltpu.make_async_remote_copy(
+            src_ref=src,
+            dst_ref=tokens.at[slot],
+            send_sem=block_send.at[slot],
+            recv_sem=block_recv.at[slot],
+            device_id={"ep": chip * CORES + other},
+        )
+
+    loop(chips - 1, lambda turn: chip_copy(chip_at(turn)).start())
+
     @pl.when(chip < chips - 1)
     def _():
         up_copy(kv_ref, me).start()
 
+    reach = chips // 2
+    far_count = jnp.maximum(chips - 1 - reach - chip, 0)
+    loop(far_count, lambda turn: far_copy(chips - 1 - turn).start())
+
     @pl.when(core == 0)
     def _():
         side_copy(kv_ref, me).start()
+
+    block_copy(normed_ref, me).start()
+    own_copy = pltpu.make_async_copy(normed_ref, tokens.at[me], own_sem)
+    own_copy.start()
+
+    def spread_pieces(turn):
+        slot = chip_at(turn) * CORES + core
+        plane_copy(slot, tp_me, tp_me).wait_recv()
+        loop(tp_count - 1, lambda way: plane_copy(slot, tp_me, tp_at(way)).start())
+
+    def share_blocks(turn):
+        slot = chip_at(turn) * CORES + core
+        loop(tp_count - 1, lambda way: plane_copy(slot, tp_at(way), tp_me).wait_recv())
+        block_copy(tokens.at[slot], slot).start()
 
     ones = jnp.ones((rows, LANES), jnp.bfloat16)
 
@@ -124,21 +201,32 @@
             lax.fori_loop(0, tiles, one_tile, 0)
 
     block_step(me, kv_ref, True)
+    loop(chips - 1, spread_pieces)
+
+    @pl.when(me == 0)
+    def _():
+        loop(chips - 1, share_blocks)
 
     def remote_step(step, carry):
         turn = step - core + 2
         own_core = turn % 2 == 0
-        slot = (chip - turn // 2) * CORES + jnp.where(own_core, core, other)
+        order = turn // 2
+        back = jnp.where(order < 2, order, chip + 2 - order)
+        slot = (chip - back) * CORES + jnp.where(own_core, core, other)
         landed = held.at[slot]
         side_copy(landed, slot).wait_recv()
 
-        @pl.when(jnp.logical_and(own_core, chip < chips - 1))
+        @pl.when(jnp.logical_and(own_core, jnp.logical_and(chip < chips - 1, back < reach)))
         def _():
             up_copy(landed, slot).start()
 
         @pl.when(own_core)
         def _():
             side_copy(landed, slot).start()
+
+        @pl.when(step == jnp.maximum(me - 2, 0))
+        def _():
+            loop(chips - 1, share_blocks)
 
         block_step(slot, landed, False)
         return carry
@@ -151,10 +239,10 @@
         whole = acc[head, :, :LANES] / acc[head, :, LANES:]
         out_ref[:, head * HEAD : (head + 1) * HEAD] = whole[:, spot].astype(out_ref.dtype)
 
-    def finish(step, carry):
+    def finish(step):
         slot = (chip - step) * CORES + core
 
-        @pl.when(chip < chips - 1)
+        @pl.when(jnp.logical_and(chip < chips - 1, step < reach))
         def _():
             up_copy(held.at[slot], slot).wait_send()
 
@@ -162,16 +250,88 @@
         def _():
             side_copy(held.at[slot], slot).wait_send()
 
-        return carry
-
-    lax.fori_loop(0, chip + 1, finish, 0)
+    loop(chip + 1, finish)
+    loop(far_count, lambda turn: far_copy(chips - 1 - turn).wait_send())
 
     @pl.when(core == 0)
     def _():
         side_copy(kv_ref, me).wait_send()
 
-
-def attention(query_rows, key_rows, value_rows, cum_gate):
+    def finish_tokens(turn):
+        target = chip_at(turn)
+        slot = target * CORES + core
+        chip_copy(target).wait_send()
+        loop(tp_count - 1, lambda way: plane_copy(slot, tp_me, tp_at(way)).wait_send())
+        block_copy(tokens.at[slot], slot).wait_send()
+
+    loop(chips - 1, finish_tokens)
+    block_copy(normed_ref, me).wait_send()
+
+    def finish_blocks(index):
+        slot = index * CORES + other
+        block_copy(tokens.at[slot], slot).wait_recv()
+
+    loop(chips, finish_blocks)
+    own_copy.wait()
+
+
+def exchange_kernel(count, *refs):
+    sources, targets = refs[:count], refs[count : 2 * count]
+    send_sem, recv_sem, own_sem = refs[2 * count :]
+    tp_count = lax.axis_size("tp")
+    tp_me = lax.axis_index("tp")
+    barrier = pltpu.get_barrier_semaphore()
+    ways = [lax.rem(tp_me + turn, tp_count) for turn in range(1, tp_count)]
+    for way in ways:
+        pl.semaphore_signal(barrier, inc=1, device_id={"tp": way})
+    pl.semaphore_wait(barrier, tp_count - 1)
+
+    def copy(index, way, owner):
+        return pltpu.make_async_remote_copy(
+            src_ref=sources[index],
+            dst_ref=targets[index].at[owner],
+            send_sem=send_sem.at[index, way],
+            recv_sem=recv_sem.at[index, owner],
+            device_id={"tp": way},
+        )
+
+    for index in range(count):
+        for way in ways:
+            copy(index, way, tp_me).start()
+    own = [
+        pltpu.make_async_copy(sources[index], targets[index].at[tp_me], own_sem.at[index])
+        for index in range(count)
+    ]
+    for one in own:
+        one.start()
+    for one in own:
+        one.wait()
+    for index in range(count):
+        for way in ways:
+            copy(index, way, way).wait_recv()
+            copy(index, way, tp_me).wait_send()
+
+
+def exchange(*arrays):
+    tp_count = lax.axis_size("tp")
+    count = len(arrays)
+    return pl.pallas_call(
+        functools.partial(exchange_kernel, count),
+        out_shape=[jax.ShapeDtypeStruct((tp_count,) + a.shape, a.dtype) for a in arrays],
+        in_specs=[pl.BlockSpec(memory_space=pltpu.VMEM)] * count,
+        out_specs=[pl.BlockSpec(memory_space=pltpu.VMEM)] * count,
+        scratch_shapes=[
+            pltpu.SemaphoreType.DMA((count, tp_count)),
+            pltpu.SemaphoreType.DMA((count, tp_count)),
+            pltpu.SemaphoreType.DMA((count,)),
+        ],
+        compiler_params=pltpu.CompilerParams(collective_id=1, has_side_effects=True),
+        cost_estimate=pl.CostEstimate(flops=0, bytes_accessed=24 * 1024 * 1024, transcendentals=0),
+        name="exchange",
+    )(*arrays)
+
+
+def attention(query_rows, key_rows, value_rows, cum_gate, normed):
     rows, width = query_rows.shape
     heads = width // HEAD
     pairs = (heads + 1) // 2
@@ -207,9 +367,15 @@
     blocks = ep_count * rows * rows * heads
     return pl.pallas_call(
         functools.partial(attention_kernel, heads),
-        out_shape=jax.ShapeDtypeStruct((rows, heads * HEAD), jnp.bfloat16),
-        in_specs=[pl.BlockSpec(memory_space=pltpu.VMEM)] * 3,
-        out_specs=pl.BlockSpec(memory_space=pltpu.VMEM),
+        out_shape=[
+            jax.ShapeDtypeStruct((rows, heads * HEAD), jnp.bfloat16),
+            jax.ShapeDtypeStruct((ep_count,) + normed.shape, jnp.bfloat16),
+        ],
+        in_specs=[pl.BlockSpec(memory_space=pltpu.VMEM)] * 4,
+        out_specs=[
+            pl.BlockSpec(memory_space=pltpu.VMEM),
+            pl.BlockSpec(memory_space=pl.ANY),
+        ],
         scratch_shapes=[
             pltpu.VMEM((ep_count, rows, 2 * padded), jnp.bfloat16),
             pltpu.VMEM((heads, rows, 2 * LANES), jnp.float32),
@@ -217,6 +383,12 @@
             pltpu.SemaphoreType.DMA((ep_count,)),
             pltpu.SemaphoreType.DMA((ep_count,)),
             pltpu.SemaphoreType.DMA((ep_count,)),
+            pltpu.SemaphoreType.DMA((ep_count,)),
+            pltpu.SemaphoreType.DMA((ep_count, lax.axis_size("tp"))),
+            pltpu.SemaphoreType.DMA((ep_count, lax.axis_size("tp"))),
+            pltpu.SemaphoreType.DMA((ep_count,)),
+            pltpu.SemaphoreType.DMA((ep_count,)),
+            pltpu.SemaphoreType.DMA,
         ],
         compiler_params=pltpu.CompilerParams(
             collective_id=0, has_side_effects=True, vmem_limit_bytes=48 * 1024 * 1024
@@ -225,7 +397,7 @@
             flops=blocks * 2 * 512, bytes_accessed=8 * 1024 * 1024, transcendentals=blocks
         ),
         name="attend",
-    )(queries, key_value, gates)
+    )(queries, key_value, gates, normed)
 
 
 def local(
@@ -245,7 +417,6 @@
     shared_up,
     shared_down,
 ):
-    heads_out = attention(query_rows, key_rows, value_rows, cum_gate)
     token_count = moe_input.shape[0]
     top_count = routes.shape[1]
     local_experts = expert_gate.shape[0]
@@ -270,23 +441,32 @@
     ranks = jnp.where(named, ranks.astype(jnp.int32), -1)
     slots = jnp.arange(capacity, dtype=jnp.int32)
     place = ranks[:, :, None] == slots[None, None, :]
-    pick = place.astype(jnp.bfloat16).reshape(token_count, expert_count * capacity)
-    own_columns = lax.dynamic_slice_in_dim(normed, first_column, column_count, 1)
-    outgoing = lax.dot_general(
-        pick, own_columns, (((0,), (0,)), ((), ())), preferred_element_type=jnp.float32
-    ).astype(jnp.bfloat16)
-    outgoing = outgoing.reshape(ep_count, local_experts, capacity, column_count)
-    arrived = lax.all_to_all(outgoing, "ep", split_axis=0, concat_axis=0, tiled=True)
-    arrived = lax.all_gather(arrived, "tp", axis=3, tiled=True)
+    heads_out, tokens = attention(query_rows, key_rows, value_rows, cum_gate, normed)
+    all_ranks = lax.all_gather(
+        ranks.astype(jnp.bfloat16).reshape(token_count, ep_count, local_experts), "ep", axis=0
+    )
+    mine = lax.dynamic_index_in_dim(all_ranks, lax.axis_index("ep"), 2, keepdims=False)
+    pick = mine.transpose(0, 2, 1)[:, :, None, :] == slots.astype(jnp.bfloat16)[None, None, :, None]
+    pick = pick.astype(jnp.bfloat16).reshape(ep_count, local_experts * capacity, token_count)
+    arrived = jnp.einsum("ast,atd->asd", pick, tokens, preferred_element_type=jnp.float32)
+    arrived = arrived.astype(jnp.bfloat16).reshape(ep_count, local_experts, capacity, -1)
     gate_val = jnp.einsum(
         "aecd,edf->aecf", arrived, expert_gate, preferred_element_type=jnp.float32
     )
     up_val = jnp.einsum("aecd,edf->aecf", arrived, expert_up, preferred_element_type=jnp.float32)
     hidden = (jax.nn.silu(gate_val) * up_val).astype(jnp.bfloat16)
-    hidden = lax.all_gather(hidden, "tp", axis=3, tiled=True)
-    result = jnp.einsum(
-        "aecf,efd->aecd", hidden, expert_down, preferred_element_type=jnp.float32
+    shared_hidden = (
+        jax.nn.silu(jnp.dot(normed, shared_gate, preferred_element_type=jnp.float32))
+        * jnp.dot(normed, shared_up, preferred_element_type=jnp.float32)
     ).astype(jnp.bfloat16)
+    slot_count = ep_count * local_experts * capacity
+    by_expert = hidden.transpose(1, 0, 2, 3).reshape(slot_count, hidden.shape[3])
+    hidden, shared_all = exchange(by_expert, shared_hidden)
+    hidden = hidden.transpose(1, 0, 2).reshape(local_experts, ep_count * capacity, -1)
+    shared_all = shared_all.transpose(1, 0, 2).reshape(token_count, -1)
+    result = jnp.einsum("esf,efd->esd", hidden, expert_down, preferred_element_type=jnp.float32)
+    result = result.astype(jnp.bfloat16).reshape(local_experts, ep_count, capacity, column_count)
+    result = result.transpose(1, 0, 2, 3)
     returned = lax.all_to_all(result, "ep", split_axis=0, concat_axis=0, tiled=True)
     returned = returned.reshape(expert_count * capacity, column_count)
     weight_high = lax.reduce_precision(weight_of, 8, 7)
@@ -299,14 +479,7 @@
             returned,
             preferred_element_type=jnp.float32,
         )
-    shared_hidden = (
-        jax.nn.silu(jnp.dot(normed, shared_gate, preferred_element_type=jnp.float32))
-        * jnp.dot(normed, shared_up, preferred_element_type=jnp.float32)
-    ).astype(jnp.bfloat16)
-    heads_all, shared_all = (
-        lax.all_gather(heads_out, "tp", axis=1, tiled=True),
-        lax.all_gather(shared_hidden, "tp", axis=1, tiled=True),
-    )
+    heads_all = lax.all_gather(heads_out, "tp", axis=1, tiled=True)
     mixer_sum = jnp.dot(heads_all, out_weight, preferred_element_type=jnp.float32)
     moe_total = routed + jnp.dot(shared_all, shared_down, preferred_element_type=jnp.float32)
     return (mixer_sum.astype(jnp.bfloat16), moe_total.astype(jnp.bfloat16))

time: 246 us -> 222 us (0.902)
  Pallas kernels: 19.1 us -> 74.3 us
  waiting for transfers between devices: 62.1 us -> 23.5 us
  blocking collectives: 46.3 us -> 15.7 us
  starting transfers between devices: 47.4 us -> 39.2 us
    all_gather x3 -> x1, waiting for transfers between devices: 59.9 us -> 0.01 us  [local(): heads_all = lax.all_gather(heads_out, 'tp', axis=1, tiled=True)]
    pallas_call x1 -> x2, Pallas kernels: 19.1 us -> 74.3 us  [the longest x1 54 us: attention(): pl.pallas_call(functools.partial(attention_kernel, heads), out_shape=[jax...]
    all_to_all x1 -> x0, blocking collectives: 35.5 us -> none  [local(): lax.all_to_all(outgoing, 'ep', split_axis=0, concat_axis=0, tiled=True)]
    all_to_all x1, waiting for transfers between devices: 2.15 us -> 22.8 us  [local(): lax.all_to_all(result, 'ep', split_axis=0, concat_axis=0, tiled=True)]
    all_to_all x1, starting transfers between devices: 47.3 us -> 39.2 us  [local(): lax.all_to_all(result, 'ep', split_axis=0, concat_axis=0, tiled=True)]
    transpose x0 -> x1, local copies, waits for them, and re-layouts: none -> 5.97 us  [local(): hidden.transpose(1, 0, 2).reshape(local_experts, ep_count * capacity, -1)]
    all_gather x1, blocking collectives: 10.7 us -> 15.7 us  [local(): lax.all_gather(ranks.astype(jnp.bfloat16).reshape(token_count, ep_count,...]
    unnamed x30 -> x25, local copies, waits for them, and re-layouts: 5.25 us -> 0.86 us
  transfers between devices with their start and end apart: 4 -> 2, of which waited for: 4 -> 1; matrix products, arithmetic and copies ran while one was open for 11% -> 6% of each run, Pallas kernels for 8% -> 0%
where the time goes in v2:
time: 222 us; the launch traced here: 221 us
  Pallas kernels  74.3 us (33%)
  starting transfers between devices  39.2 us (18%)
  local copies, waits for them, and re-layouts  28.5 us (13%)
  waiting for transfers between devices  23.5 us (11%)
  matrix products  19.1 us (9%)
  blocking collectives  15.7 us (7%)
  between operations  14.4 us (6%)
  other arithmetic  6.32 us (3%)
    pallas_call x1, Pallas kernels, attention(): pl.pallas_call(functools.partial(attention_kernel, heads), out_shape=[jax...  54 us
    all_to_all x1, starting transfers between devices, local(): lax.all_to_all(result, 'ep', split_axis=0, concat_axis=0, tiled=True)  39.2 us
    all_to_all x1, waiting for transfers between devices, local(): lax.all_to_all(result, 'ep', split_axis=0, concat_axis=0, tiled=True)  22.8 us
    pallas_call x1, Pallas kernels, exchange(): pl.pallas_call(functools.partial(exchange_kernel, count), out_shape=[jax....  20.3 us
    all_gather x1, blocking collectives, local(): lax.all_gather(ranks.astype(jnp.bfloat16).reshape(token_count, ep_count,...  15.7 us
    transpose x1, local copies, waits for them, and re-layouts, local(): hidden.transpose(1, 0, 2).reshape(local_experts, ep_count * capacity, -1)  5.97 us
    reshape x1, local copies, waits for them, and re-layouts, attention(): gates = terms.reshape(pairs * LANES, cum_gate.shape[1]).T  4.81 us
  transfers between devices with their start and end apart: 2, of which 1 were waited for; matrix products, arithmetic and copies ran while one was open for 6% of the time, Pallas kernels for 0%

profile of v2, /device:TPU:0, one launch (start us, length us, event | category | flops | bytes accessed | tf_op | source)
XLA Modules:
  0.0 221.1 jit_solution(4224782173161312023)
XLA Ops:
  7.2 0.0 copy-start
  7.3 1.2 broadcast_multiply_fusion
  8.5 1.0 fusion.21
  9.4 0.1 pad_maximum_fusion.2
  9.5 0.1 copy.59
  9.7 0.1 convert_element_type.93
  9.8 2.0 pad.4
  11.8 4.8 %copy.72 = bf16[256,6144]{0,1:T(8,128)(2,1)} copy(bf16[256,6144]{1,0:T(8,128)(2,1)} %bitcast.75) | data formatting | bytes 6291456 | tf_op jit(solution)/shard_map/reshape | solution.py:366
  16.6 0.2 fusion.4
  16.9 0.2 fusion.24
  17.1 15.7 %all_gather.7 = bf16[8,192,8,4]{1,2,3,0:T(8,128)(2,1)S(1)} all-gather(bf16[1,192,8,4]{1,2,3,0:T(8,128)(2,1)S(1)} %copy.61), channel_id=1, replica_groups=mesh['ep'=8,'tp'=4] {'ep'}, dimensions={0}, use_global_device_ids=true | all-gather | bytes 110592 | tf_op jit(solution)/shard_map/all_gather | solution.py:445
  32.9 0.1 eq.107
  33.0 1.5 fusion.6.normed_ref
  34.5 0.1 pad_maximum_fusion.1.kv_ref
  34.6 0.3 bitcast_compare_fusion
  34.8 0.1 broadcast_select_fusion.3
  34.9 0.2 maximum_bitcast_fusion
  35.1 0.2 pad_maximum_fusion.q_ref
  35.3 54.0 %attend.1 = (bf16[768,256]{1,0:T(8,128)(2,1)}, bf16[8,192,2048]{2,1,0:T(8,128)(2,1)}) custom-call(bf16[4,768,256]{2,1,0:T(8,128)(2,1)S(1)} %pad_maximum_fusion.q_ref, bf16[768,512]{1,0:T(8,128)(2,1)S(1)} %pad_maximum_fusion.1.kv_ref, bf16[6144,256]{1,0:T(8,128)(2,1)} %bitcast.77, bf16[192,2048]{1,0:T(8,128)(2,1)S(1)} %fusion.6.normed_ref), custom_call_target="tpu_custom_call" | custom-call | flops 19327352832 | bytes 8388608 | tf_op jit(solution)/shard_map/attend/pallas_call | solution.py:368
  89.4 4.2 %convolution_convert_fusion = bf16[8,144,2048]{2,1,0:T(8,128)(2,1)S(1)} fusion(bf16[8,192,2048]{2,1,0:T(8,128)(2,1)} %get-tuple-element.7, pred[8,144,192]{2,0,1:T(8,128)(4,1)S(1)} %bitcast_compare_fusion), kind=kOutput, calls=%fused_computation | convolution fusion | flops 908328960 | bytes 11231232 | tf_op jit(solution)/shard_map/ast,atd->asd/dot_general | solution.py:451
  93.5 2.6 %copy.64 = bf16[8,144,2048]{2,0,1:T(8,128)(2,1)S(1)} copy(bf16[8,144,2048]{2,1,0:T(8,128)(2,1)S(1)} %convolution_convert_fusion) | data formatting | bytes 9437184 | tf_op jit(solution)/shard_map/convert_element_type | solution.py:452
  96.2 1.4 fusion.2
  97.5 0.2 copy-done.11
  97.7 1.4 fusion.10
  99.1 0.1 copy.65
  99.2 0.8 reshape.147.refs_0_
  100.0 1.4 fusion.25
  101.4 2.0 fusion.15.refs_1_
  103.4 20.3 %exchange.1 = (bf16[4,1152,128]{2,1,0:T(8,128)(2,1)}, bf16[4,192,128]{2,1,0:T(8,128)(2,1)}) custom-call(bf16[1152,128]{1,0:T(8,128)(2,1)} %reshape.147.refs_0_, bf16[192,128]{1,0:T(8,128)(2,1)} %fusion.15.refs_1_), custom_call_target="tpu_custom_call" | custom-call | bytes 25165824 | tf_op jit(solution)/shard_map/exchange/pallas_call | solution.py:318
  123.7 6.0 %copy.66 = bf16[1152,4,128]{2,1,0:T(4,128)(2,1)S(1)} copy(bf16[1152,4,128]{2,0,1:T(8,128)(2,1)} %bitcast.78) | data formatting | bytes 2359296 | tf_op jit(solution)/shard_map/transpose | solution.py:465
  129.7 1.3 reshape.148
  131.0 2.0 convolution_convert_fusion.1
  133.0 1.9 copy.67
  135.0 39.2 %all-to-all-start = ((bf16[8,4,36,512]{3,1,2,0:T(4,128)(2,1)}), bf16[8,4,36,512]{3,1,2,0:T(4,128)(2,1)S(1)}, u32[]{:S(2)}, u32[]{:S(2)}) async-start(bf16[8,4,36,512]{3,1,2,0:T(4,128)(2,1)} %bitcast.76), calls=%async_computation | async-start | bytes 2359296 | tf_op jit(solution)/shard_map/all_to_all | solution.py:470
  174.1 0.0 all-gather.2.cloned.1.call-start
  174.2 0.7 all-gather.2.cloned.1.call-update
  174.9 1.5 select_convert_fusion
  176.4 2.1 convert_element_type.99
  178.6 2.1 convert_element_type.107
  180.7 22.8 %all-to-all-done = bf16[8,4,36,512]{3,1,2,0:T(4,128)(2,1)S(1)} async-done(((bf16[8,4,36,512]{3,1,2,0:T(4,128)(2,1)}), bf16[8,4,36,512]{3,1,2,0:T(4,128)(2,1)S(1)}, u32[]{:S(2)}, u32[]{:S(2)}) %all-to-all-start) | async-done | bytes 1179680 | tf_op jit(solution)/shard_map/all_to_all | solution.py:470
  203.5 1.3 copy.68
  204.9 2.1 reshape.150
  207.0 1.6 fusion.26
  208.6 0.5 convolution_add_fusion.1
  209.1 0.6 copy-done.4
  209.7 0.0 copy-done.7
  209.7 0.9 fusion.14
  210.6 3.6 %convolution_convert_fusion.2 = bf16[768,512]{1,0:T(8,128)(2,1)} fusion(bf16[768,1024]{1,0:T(8,128)(2,1)} %all-gather.2.cloned.1.call-done, bf16[1024,512]{1,0:T(8,128)(2,1)} %param.19), kind=kOutput, calls=%fused_computation.12 | convolution fusion | flops 805699584 | bytes 3407872 | tf_op jit(solution)/shard_map/dot_general | solution.py:483
  (37 shorter events, 0.2 us)
Async XLA Ops:
  7.2 123.8 %copy-start = (bf16[4,512,512]{2,1,0:T(8,128)(2,1)S(1)}, bf16[4,512,512]{2,1,0:T(8,128)(2,1)}, u32[]{:S(2)}) copy-start(bf16[4,512,512]{2,1,0:T(8,128)(2,1)} %param.26) | copy-start | bytes 6291460
  11.8 4.8 %copy-start.2 = (bf16[192,2048]{1,0:T(8,128)(2,1)S(1)}, bf16[192,2048]{1,0:T(8,128)(2,1)}, u32[]{:S(2)}) copy-start(bf16[192,2048]{1,0:T(8,128)(2,1)} %param.20) | copy-start | bytes 2359300
  11.8 5.1 %copy-start.8 = (s32[192,3]{0,1:T(4,128)S(1)}, s32[192,3]{0,1:T(4,128)}, u32[]{:S(2)}) copy-start(s32[192,3]{0,1:T(4,128)} %param.22) | copy-start | bytes 6916
  11.8 21.2 %copy-start.9 = (f32[2048]{0:T(1024)S(1)}, f32[2048]{0:T(1024)}, u32[]{:S(2)}) copy-start(f32[2048]{0:T(1024)} %param.21) | copy-start | bytes 24580
  33.0 1.5 copy-start.5
  33.0 1.5 copy-start.6
  93.5 2.6 %copy-start.1 = (bf16[4,2048,128]{2,1,0:T(8,128)(2,1)S(1)}, bf16[4,2048,128]{2,1,0:T(8,128)(2,1)}, u32[]{:S(2)}) copy-start(bf16[4,2048,128]{2,1,0:T(8,128)(2,1)} %param.24) | copy-start | bytes 6291460
  96.1 1.6 copy-start.11
  135.0 39.9 %copy-start.10 = (f32[192,3]{0,1:T(4,128)S(1)}, f32[192,3]{0,1:T(4,128)}, u32[]{:S(2)}) copy-start(f32[192,3]{0,1:T(4,128)} %param.23) | copy-start | bytes 6916
  135.0 68.6 %all-to-all-start = ((bf16[8,4,36,512]{3,1,2,0:T(4,128)(2,1)}), bf16[8,4,36,512]{3,1,2,0:T(4,128)(2,1)S(1)}, u32[]{:S(2)}, u32[]{:S(2)}) async-start(bf16[8,4,36,512]{3,1,2,0:T(4,128)(2,1)} %bitcast.76), calls=%async_computation | async-start | bytes 2359296 | tf_op jit(solution)/shard_map/all_to_all | solution.py:470
  174.1 36.5 %all-gather.2.cloned.1.call-start = ((), (), s32[]{:S(2)}) async-start(), calls=%async_computation.1 | async-start | bytes 1966080 | tf_op jit(solution)/shard_map/all_gather | solution.py:482
  207.0 1.6 copy-start.3
  208.6 1.0 copy-start.4
  208.6 1.1 copy-start.7
Sparse Core Ops, SparseCore 0:
  176.8 32.0 all-gather.1

commit v3 on v2

--- a/solution.py
+++ b/solution.py
@@ -21,8 +21,10 @@
     kv_ref,
     gate_ref,
     normed_ref,
+    rank_ref,
     out_ref,
     tokens,
+    picks,
     held,
     acc,
     row_max,
@@ -35,6 +37,8 @@
     block_send,
     block_recv,
     own_sem,
+    rank_send,
+    rank_recv,
 ):
     rows = kv_ref.shape[0]
     width = kv_ref.shape[1] // 2
@@ -69,10 +73,23 @@
     def tp_at(turn):
         return lax.rem(tp_me + turn + 1, tp_count)
 
-    greet(ep=chip * CORES + other)
-    loop(chips - 1, lambda turn: greet(ep=chip_at(turn) * CORES + core))
+    ep_count = chips * CORES
+
+    def ep_at(turn):
+        return lax.rem(me + turn + 1, ep_count)
+
+    loop(ep_count - 1, lambda turn: greet(ep=ep_at(turn)))
     loop(tp_count - 1, lambda turn: greet(tp=tp_at(turn)))
-    pl.semaphore_wait(barrier, chips + tp_count - 1)
+    pl.semaphore_wait(barrier, ep_count + tp_count - 2)
+
+    def rank_copy(target, owner):
+        return pltpu.make_async_remote_copy(
+            src_ref=rank_ref.at[target],
+            dst_ref=picks.at[owner],
+            send_sem=rank_send.at[target],
+            recv_sem=rank_recv.at[owner],
+            device_id={"ep": target},
+        )
 
     def up_copy(src, slot):
         return pltpu.make_async_remote_copy(
@@ -149,6 +166,8 @@
     block_copy(normed_ref, me).start()
     own_copy = pltpu.make_async_copy(normed_ref, tokens.at[me], own_sem)
     own_copy.start()
+    loop(ep_count - 1, lambda turn: rank_copy(ep_at(turn), me).start())
+    picks[me] = rank_ref[me]
 
     def spread_pieces(turn):
         slot = chip_at(turn) * CORES + core
@@ -274,6 +293,12 @@
     loop(chips, finish_blocks)
     own_copy.wait()
 
+    def finish_ranks(turn):
+        rank_copy(ep_at(turn), me).wait_send()
+        rank_copy(ep_at(turn), ep_at(turn)).wait_recv()
+
+    loop(ep_count - 1, finish_ranks)
+
 
 def exchange_kernel(count, *refs):
     sources, targets = refs[:count], refs[count : 2 * count]
@@ -286,10 +311,16 @@
         pl.semaphore_signal(barrier, inc=1, device_id={"tp": way})
     pl.semaphore_wait(barrier, tp_count - 1)
 
+    def place(index, owner):
+        span = sources[index].shape[1]
+        if span % LANES:
+            return targets[index].at[owner]
+        return targets[index].at[:, pl.ds(pl.multiple_of(owner * span, span), span)]
+
     def copy(index, way, owner):
         return pltpu.make_async_remote_copy(
             src_ref=sources[index],
-            dst_ref=targets[index].at[owner],
+            dst_ref=place(index, owner),
             send_sem=send_sem.at[index, way],
             recv_sem=recv_sem.at[index, owner],
             device_id={"tp": way},
@@ -299,7 +330,7 @@
         for way in ways:
             copy(index, way, tp_me).start()
     own = [
-        pltpu.make_async_copy(sources[index], targets[index].at[tp_me], own_sem.at[index])
+        pltpu.make_async_copy(sources[index], place(index, tp_me), own_sem.at[index])
         for index in range(count)
     ]
     for one in own:
@@ -312,12 +343,18 @@
             copy(index, way, tp_me).wait_send()
 
 
-def exchange(*arrays):
+def exchange(collective_id, *arrays):
     tp_count = lax.axis_size("tp")
     count = len(arrays)
-    return pl.pallas_call(
+
+    def gathered(a):
+        rows, span = a.shape
+        shape = (tp_count, rows, span) if span % LANES else (rows, tp_count * span)
+        return jax.ShapeDtypeStruct(shape, a.dtype)
+
+    results = pl.pallas_call(
         functools.partial(exchange_kernel, count),
-        out_shape=[jax.ShapeDtypeStruct((tp_count,) + a.shape, a.dtype) for a in arrays],
+        out_shape=[gathered(a) for a in arrays],
         in_specs=[pl.BlockSpec(memory_space=pltpu.VMEM)] * count,
         out_specs=[pl.BlockSpec(memory_space=pltpu.VMEM)] * count,
         scratch_shapes=[
@@ -325,13 +362,16 @@
             pltpu.SemaphoreType.DMA((count, tp_count)),
             pltpu.SemaphoreType.DMA((count,)),
         ],
-        compiler_params=pltpu.CompilerParams(collective_id=1, has_side_effects=True),
+        compiler_params=pltpu.CompilerParams(collective_id=collective_id, has_side_effects=True),
         cost_estimate=pl.CostEstimate(flops=0, bytes_accessed=24 * 1024 * 1024, transcendentals=0),
         name="exchange",
     )(*arrays)
-
-
-def attention(query_rows, key_rows, value_rows, cum_gate, normed):
+    return [
+        r if r.ndim == 2 else r.transpose(1, 0, 2).reshape(r.shape[1], -1) for r in results
+    ]
+
+
+def attention(query_rows, key_rows, value_rows, cum_gate, normed, ranks):
     rows, width = query_rows.shape
     heads = width // HEAD
     pairs = (heads + 1) // 2
@@ -358,23 +398,26 @@
     rest = minus - high
     mid = lax.reduce_precision(rest, 8, 7)
     low = rest - mid
-    terms = jnp.stack([high, mid, low], axis=1).astype(jnp.bfloat16)
-    if heads % 2:
-        terms = jnp.concatenate([terms, jnp.zeros_like(terms[:1])], axis=0)
-    terms = terms.reshape(pairs, 6, cum_gate.shape[1])
-    terms = jnp.pad(terms, ((0, 0), (0, LANES - 6), (0, 0)))
-    gates = terms.reshape(pairs * LANES, cum_gate.shape[1]).T
+    terms = jnp.concatenate([high, mid, low], axis=0).astype(jnp.bfloat16)
+    source = jnp.arange(3 * heads)
+    spot = (source % heads // 2) * LANES + (source % heads % 2) * 3 + source // heads
+    layout = (spot[:, None] == jnp.arange(padded)[None, :]).astype(jnp.bfloat16)
+    gates = lax.dot_general(
+        terms, layout, (((0,), (0,)), ((), ())), preferred_element_type=jnp.float32
+    ).astype(jnp.bfloat16)
     blocks = ep_count * rows * rows * heads
     return pl.pallas_call(
         functools.partial(attention_kernel, heads),
         out_shape=[
             jax.ShapeDtypeStruct((rows, heads * HEAD), jnp.bfloat16),
             jax.ShapeDtypeStruct((ep_count,) + normed.shape, jnp.bfloat16),
+            jax.ShapeDtypeStruct(ranks.shape, jnp.bfloat16),
         ],
-        in_specs=[pl.BlockSpec(memory_space=pltpu.VMEM)] * 4,
+        in_specs=[pl.BlockSpec(memory_space=pltpu.VMEM)] * 5,
         out_specs=[
             pl.BlockSpec(memory_space=pltpu.VMEM),
             pl.BlockSpec(memory_space=pl.ANY),
+            pl.BlockSpec(memory_space=pltpu.VMEM),
         ],
         scratch_shapes=[
             pltpu.VMEM((ep_count, rows, 2 * padded), jnp.bfloat16),
@@ -389,6 +432,8 @@
             pltpu.SemaphoreType.DMA((ep_count,)),
             pltpu.SemaphoreType.DMA((ep_count,)),
             pltpu.SemaphoreType.DMA,
+            pltpu.SemaphoreType.DMA((ep_count,)),
+            pltpu.SemaphoreType.DMA((ep_count,)),
         ],
         compiler_params=pltpu.CompilerParams(
             collective_id=0, has_side_effects=True, vmem_limit_bytes=48 * 1024 * 1024
@@ -397,7 +442,7 @@
             flops=blocks * 2 * 512, bytes_accessed=8 * 1024 * 1024, transcendentals=blocks
         ),
         name="attend",
-    )(queries, key_value, gates, normed)
+    )(queries, key_value, gates, normed, ranks)
 
 
 def local(
@@ -441,12 +486,11 @@
     ranks = jnp.where(named, ranks.astype(jnp.int32), -1)
     slots = jnp.arange(capacity, dtype=jnp.int32)
     place = ranks[:, :, None] == slots[None, None, :]
-    heads_out, tokens = attention(query_rows, key_rows, value_rows, cum_gate, normed)
-    all_ranks = lax.all_gather(
-        ranks.astype(jnp.bfloat16).reshape(token_count, ep_count, local_experts), "ep", axis=0
+    rank_rows = ranks.astype(jnp.bfloat16).T.reshape(ep_count, local_experts, token_count)
+    heads_out, tokens, mine = attention(
+        query_rows, key_rows, value_rows, cum_gate, normed, rank_rows
     )
-    mine = lax.dynamic_index_in_dim(all_ranks, lax.axis_index("ep"), 2, keepdims=False)
-    pick = mine.transpose(0, 2, 1)[:, :, None, :] == slots.astype(jnp.bfloat16)[None, None, :, None]
+    pick = mine[:, :, None, :] == slots.astype(jnp.bfloat16)[None, None, :, None]
     pick = pick.astype(jnp.bfloat16).reshape(ep_count, local_experts * capacity, token_count)
     arrived = jnp.einsum("ast,atd->asd", pick, tokens, preferred_element_type=jnp.float32)
     arrived = arrived.astype(jnp.bfloat16).reshape(ep_count, local_experts, capacity, -1)
@@ -461,12 +505,12 @@
     ).astype(jnp.bfloat16)
     slot_count = ep_count * local_experts * capacity
     by_expert = hidden.transpose(1, 0, 2, 3).reshape(slot_count, hidden.shape[3])
-    hidden, shared_all = exchange(by_expert, shared_hidden)
-    hidden = hidden.transpose(1, 0, 2).reshape(local_experts, ep_count * capacity, -1)
-    shared_all = shared_all.transpose(1, 0, 2).reshape(token_count, -1)
+    hidden, shared_all = exchange(1, by_expert, shared_hidden)
+    hidden = hidden.reshape(local_experts, ep_count * capacity, -1)
     result = jnp.einsum("esf,efd->esd", hidden, expert_down, preferred_element_type=jnp.float32)
     result = result.astype(jnp.bfloat16).reshape(local_experts, ep_count, capacity, column_count)
     result = result.transpose(1, 0, 2, 3)
+    result, heads_out = lax.optimization_barrier((result, heads_out))
     returned = lax.all_to_all(result, "ep", split_axis=0, concat_axis=0, tiled=True)
     returned = returned.reshape(expert_count * capacity, column_count)
     weight_high = lax.reduce_precision(weight_of, 8, 7)
@@ -479,7 +523,7 @@
             returned,
             preferred_element_type=jnp.float32,
         )
-    heads_all = lax.all_gather(heads_out, "tp", axis=1, tiled=True)
+    (heads_all,) = exchange(2, heads_out)
     mixer_sum = jnp.dot(heads_all, out_weight, preferred_element_type=jnp.float32)
     moe_total = routed + jnp.dot(shared_all, shared_down, preferred_element_type=jnp.float32)
     return (mixer_sum.astype(jnp.bfloat16), moe_total.astype(jnp.bfloat16))

time: 222 us -> 184 us (0.83)
  Pallas kernels: 74.3 us -> 98.6 us
  waiting for transfers between devices: 23.5 us -> 0.01 us
  blocking collectives: 15.7 us -> 0 us
  local copies, waits for them, and re-layouts: 28.5 us -> 14.8 us
  between operations: 14.4 us -> 0.99 us
  matrix products: 19.1 us -> 21.8 us
    pallas_call x1 -> x2, Pallas kernels: 20.3 us -> 43.2 us  [exchange(): pl.pallas_call(functools.partial(exchange_kernel, count), out_shape=[gath...]
    all_to_all x1, waiting for transfers between devices: 22.8 us -> 0.01 us  [local(): lax.all_to_all(result, 'ep', split_axis=0, concat_axis=0, tiled=True)]
    all_gather x1 -> x0, blocking collectives: 15.7 us -> none  [local(): lax.all_gather(ranks.astype(jnp.bfloat16).reshape(token_count, ep_count,...]
    reshape x2 -> x1, local copies, waits for them, and re-layouts: 6.11 us -> 0.01 us  [local(): ranks.astype(jnp.bfloat16).T.reshape(ep_count, local_experts, token_count)]
    transpose x1 -> x0, local copies, waits for them, and re-layouts: 5.97 us -> none  [local(): hidden.transpose(1, 0, 2).reshape(local_experts, ep_count * capacity, -1)]
    dot_general x0 -> x1, matrix products: none -> 2.75 us  [attention(): lax.dot_general(terms, layout, (((0,), (0,)), ((), ())), preferred_elemen...]
  transfers between devices with their start and end apart: 2 -> 1, of which waited for: 1 -> 0; matrix products, arithmetic and copies ran while one was open for 6% -> 5% of each run, Pallas kernels for 0% -> 13%
where the time goes in v3:
time: 184 us; the launch traced here: 183 us
  Pallas kernels  98.6 us (54%)
  starting transfers between devices  39.6 us (22%)
  matrix products  21.8 us (12%)
  local copies, waits for them, and re-layouts  14.8 us (8%)
  other arithmetic  7.29 us (4%)
    pallas_call x1, Pallas kernels, attention(): pl.pallas_call(functools.partial(attention_kernel, heads), out_shape=[jax...  55.4 us
    pallas_call x2, Pallas kernels, exchange(): pl.pallas_call(functools.partial(exchange_kernel, count), out_shape=[gath...  43.2 us
    all_to_all x1, starting transfers between devices, local(): lax.all_to_all(result, 'ep', split_axis=0, concat_axis=0, tiled=True)  39.6 us
    convert_element_type x2, local copies, waits for them, and re-layouts, local(): spread = jnp.where(place, weight[:, :, None], 0.0).astype(jnp.bfloat16)  4.24 us
    dot_general x1, matrix products, local(): jnp.einsum('ast,atd->asd', pick, tokens, preferred_element_type=jnp.float32)  4.17 us
  transfers between devices with their start and end apart: 1, of which 0 were waited for; matrix products, arithmetic and copies ran while one was open for 5% of the time, Pallas kernels for 13%

profile of v3, /device:TPU:0, one launch (start us, length us, event | category | flops | bytes accessed | tf_op | source)
XLA Modules:
  0.0 183.2 jit_solution(2117989106883149727)
XLA Ops:
  0.6 0.0 copy-start
  0.6 0.0 copy-start.3
  0.7 0.0 copy-start.7
  0.8 1.2 broadcast_multiply_fusion
  2.0 1.0 reduce-precision_convert_fusion.1
  2.9 0.0 copy-done.3
  2.9 0.2 fusion.4
  3.2 0.2 fusion.16
  3.4 1.4 fusion.6.normed_ref
  4.8 1.2 pad_maximum_fusion.1.kv_ref
  6.0 0.1 broadcast_select_fusion.3
  6.1 0.2 maximum_bitcast_fusion
  6.3 0.2 pad_maximum_fusion.q_ref
  6.5 2.8 %convolution_convert_fusion.gate_ref = bf16[6144,256]{1,0:T(8,128)(2,1)} fusion(bf16[4,6144]{1,0:T(4,128)(2,1)S(1)} %get-tuple-element.23, bf16[4,6144]{1,0:T(4,128)(2,1)S(1)} %get-tuple-element.24, bf16[4,6144]{1,0:T(4,128)(2,1)S(1)} %get-tuple-element.22, s32[12]{0:T(128)S(1)} %fusion.25), kind=kOutput, calls=%fused_computation | convolution fusion | flops 39767040 | bytes 3293232 | tf_op jit(solution)/shard_map/dot_general | solution.py:405
  9.2 55.4 %attend.1 = (bf16[768,256]{1,0:T(8,128)(2,1)S(1)}, bf16[8,192,2048]{2,1,0:T(8,128)(2,1)}, bf16[8,4,192]{2,1,0:T(4,128)(2,1)S(1)}) custom-call(bf16[4,768,256]{2,1,0:T(8,128)(2,1)S(1)} %pad_maximum_fusion.q_ref, bf16[768,512]{1,0:T(8,128)(2,1)S(1)} %pad_maximum_fusion.1.kv_ref, bf16[6144,256]{1,0:T(8,128)(2,1)} %convolution_convert_fusion.gate_ref, ...), custom_call_target="tpu_custom_call" | custom-call | flops 19327352832 | bytes 8388608 | tf_op jit(solution)/shard_map/attend/pallas_call | solution.py:409
  64.7 0.8 copy-done.1
  65.5 0.1 eq.124
  65.6 0.3 bitcast_compare_fusion
  65.8 4.2 %convolution_convert_fusion.1 = bf16[8,144,2048]{2,1,0:T(8,128)(2,1)S(1)} fusion(bf16[8,192,2048]{2,1,0:T(8,128)(2,1)} %get-tuple-element.10, pred[8,144,192]{2,0,1:T(8,128)(4,1)S(1)} %bitcast_compare_fusion), kind=kOutput, calls=%fused_computation.1 | convolution fusion | flops 908328960 | bytes 11231232 | tf_op jit(solution)/shard_map/ast,atd->asd/dot_general | solution.py:495
  70.0 0.0 copy-start.2
  70.0 2.6 %copy.33 = bf16[8,144,2048]{2,0,1:T(8,128)(2,1)S(1)} copy(bf16[8,144,2048]{2,1,0:T(8,128)(2,1)S(1)} %convolution_convert_fusion.1) | data formatting | bytes 9437184 | tf_op jit(solution)/shard_map/convert_element_type | solution.py:496
  72.6 0.0 copy-start.10
  72.6 1.4 fusion.2
  74.0 0.2 copy-done.10
  74.2 1.4 fusion.10
  75.6 0.1 copy.34
  75.7 0.8 reshape.191.refs_0_
  76.4 1.4 fusion.29
  77.8 2.0 %fusion.15.refs_1_ = bf16[192,128]{1,0:T(8,128)(2,1)} fusion(bf16[192,2048]{1,0:T(8,128)(2,1)S(1)} %fusion.6.normed_ref, bf16[2048,128]{1,0:T(8,128)(2,1)} %param.28, f32[192,128]{1,0:T(8,128)S(1)} %fusion.29), kind=kOutput, calls=%fused_computation.24 | convolution fusion | flops 100810752 | bytes 1458176 | tf_op jit(solution)/shard_map/dot_general | solution.py:504
  79.9 20.1 %exchange.2 = (bf16[1152,512]{1,0:T(8,128)(2,1)}, bf16[192,512]{1,0:T(8,128)(2,1)}) custom-call(bf16[1152,128]{1,0:T(8,128)(2,1)} %reshape.191.refs_0_, bf16[192,128]{1,0:T(8,128)(2,1)} %fusion.15.refs_1_), custom_call_target="tpu_custom_call" | custom-call | bytes 25165824 | tf_op jit(solution)/shard_map/exchange/pallas_call | solution.py:355
  99.9 2.0 %convolution_convert_fusion.2 = bf16[4,288,512]{2,1,0:T(8,128)(2,1)S(1)} fusion(bf16[4,288,512]{2,1,0:T(8,128)(2,1)} %bitcast.56, bf16[4,512,512]{2,1,0:T(8,128)(2,1)S(1)} %copy-done), kind=kOutput, calls=%fused_computation.12 | convolution fusion | flops 604569600 | bytes 4456448 | tf_op jit(solution)/shard_map/esf,efd->esd/dot_general | solution.py:510
  102.0 1.9 %copy.35 = bf16[4,288,512]{2,0,1:T(4,128)(2,1)} copy(bf16[4,288,512]{2,1,0:T(8,128)(2,1)S(1)} %convolution_convert_fusion.2) | data formatting | bytes 2359296 | tf_op jit(solution)/shard_map/convert_element_type | solution.py:511
  103.9 39.6 %all-to-all-start = ((bf16[8,4,36,512]{3,1,2,0:T(4,128)(2,1)}), bf16[8,4,36,512]{3,1,2,0:T(4,128)(2,1)S(1)}, u32[]{:S(2)}, u32[]{:S(2)}) async-start(bf16[8,4,36,512]{3,1,2,0:T(4,128)(2,1)} %bitcast.55), calls=%async_computation | async-start | bytes 2359296 | tf_op jit(solution)/shard_map/all_to_all | solution.py:514
  143.6 1.5 select_convert_fusion
  145.1 2.1 %convert_element_type.110 = bf16[192,1152]{0,1:T(8,128)(2,1)} reshape(bf16[192,32,36]{0,2,1:T(8,128)(2,1)} %get-tuple-element.26) | data formatting | bytes 884736 | tf_op jit(solution)/shard_map/convert_element_type | solution.py:520
  147.2 2.1 %convert_element_type.112 = bf16[192,1152]{0,1:T(8,128)(2,1)} reshape(bf16[192,32,36]{0,2,1:T(8,128)(2,1)} %get-tuple-element.25) | data formatting | bytes 884736 | tf_op jit(solution)/shard_map/convert_element_type | solution.py:520
  149.4 23.1 %exchange.3 = bf16[768,1024]{1,0:T(8,128)(2,1)} custom-call(bf16[768,256]{1,0:T(8,128)(2,1)} %copy-done.1), custom_call_target="tpu_custom_call" | custom-call | bytes 25165824 | tf_op jit(solution)/shard_map/exchange/pallas_call | solution.py:355
  172.5 3.6 %convolution_convert_fusion.3 = bf16[768,512]{1,0:T(8,128)(2,1)} fusion(bf16[768,1024]{1,0:T(8,128)(2,1)} %exchange.3, bf16[1024,512]{1,0:T(8,128)(2,1)} %param.19), kind=kOutput, calls=%fused_computation.13 | convolution fusion | flops 805699584 | bytes 3407872 | tf_op jit(solution)/shard_map/dot_general | solution.py:527
  176.1 0.0 all-to-all-done
  176.1 1.4 copy.36
  177.4 2.1 %reshape.194 = bf16[1152,512]{1,0:T(8,128)(2,1)S(1)} reshape(bf16[8,4,36,512]{3,2,1,0:T(8,128)(2,1)} %copy.36) | data formatting | bytes 2359296 | tf_op jit(solution)/shard_map/reshape | solution.py:515
  179.6 1.6 fusion.30
  181.2 0.0 copy-done.4
  181.2 0.0 copy-start.5
  181.2 0.5 convolution_add_fusion.1
  181.7 0.6 copy-done.5
  182.2 0.0 copy-done.6
  182.3 1.0 fusion.14
  (26 shorter events, 0.2 us)
Async XLA Ops:
  0.6 99.3 %copy-start = (bf16[4,512,512]{2,1,0:T(8,128)(2,1)S(1)}, bf16[4,512,512]{2,1,0:T(8,128)(2,1)}, u32[]{:S(2)}) copy-start(bf16[4,512,512]{2,1,0:T(8,128)(2,1)} %param.26) | copy-start | bytes 6291460
  0.6 2.3 %copy-start.3 = (bf16[192,2048]{1,0:T(8,128)(2,1)S(1)}, bf16[192,2048]{1,0:T(8,128)(2,1)}, u32[]{:S(2)}) copy-start(bf16[192,2048]{1,0:T(8,128)(2,1)} %param.20) | copy-start | bytes 2359300
  0.7 2.5 %copy-start.7 = (s32[192,3]{0,1:T(4,128)S(1)}, s32[192,3]{0,1:T(4,128)}, u32[]{:S(2)}) copy-start(s32[192,3]{0,1:T(4,128)} %param.22) | copy-start | bytes 6916
  0.7 2.8 %copy-start.8 = (f32[2048]{0:T(1024)S(1)}, f32[2048]{0:T(1024)}, u32[]{:S(2)}) copy-start(f32[2048]{0:T(1024)} %param.21) | copy-start | bytes 24580
  64.7 0.8 copy-start.1
  70.0 2.6 %copy-start.2 = (bf16[4,2048,128]{2,1,0:T(8,128)(2,1)S(1)}, bf16[4,2048,128]{2,1,0:T(8,128)(2,1)}, u32[]{:S(2)}) copy-start(bf16[4,2048,128]{2,1,0:T(8,128)(2,1)} %param.24) | copy-start | bytes 6291460
  72.6 1.6 copy-start.10
  103.9 39.6 %copy-start.9 = (f32[192,3]{0,1:T(4,128)S(1)}, f32[192,3]{0,1:T(4,128)}, u32[]{:S(2)}) copy-start(f32[192,3]{0,1:T(4,128)} %param.23) | copy-start | bytes 6916
  103.9 72.1 %all-to-all-start = ((bf16[8,4,36,512]{3,1,2,0:T(4,128)(2,1)}), bf16[8,4,36,512]{3,1,2,0:T(4,128)(2,1)S(1)}, u32[]{:S(2)}, u32[]{:S(2)}) async-start(bf16[8,4,36,512]{3,1,2,0:T(4,128)(2,1)} %bitcast.55), calls=%async_computation | async-start | bytes 2359296 | tf_op jit(solution)/shard_map/all_to_all | solution.py:514
  179.6 1.6 copy-start.4
  181.2 1.0 copy-start.5
  181.2 1.1 copy-start.6

commit v4 on v3

--- a/solution.py
+++ b/solution.py
@@ -100,15 +100,6 @@
             device_id={"ep": me + CORES},
         )
 
-    def far_copy(target):
-        return pltpu.make_async_remote_copy(
-            src_ref=kv_ref,
-            dst_ref=held.at[me],
-            send_sem=up_send.at[target * CORES + core],
-            recv_sem=recv_sem.at[me],
-            device_id={"ep": target * CORES + core},
-        )
-
     def side_copy(src, slot):
         return pltpu.make_async_remote_copy(
             src_ref=src,
@@ -154,10 +145,6 @@
     @pl.when(chip < chips - 1)
     def _():
         up_copy(kv_ref, me).start()
-
-    reach = chips // 2
-    far_count = jnp.maximum(chips - 1 - reach - chip, 0)
-    loop(far_count, lambda turn: far_copy(chips - 1 - turn).start())
 
     @pl.when(core == 0)
     def _():
@@ -229,13 +216,11 @@
     def remote_step(step, carry):
         turn = step - core + 2
         own_core = turn % 2 == 0
-        order = turn // 2
-        back = jnp.where(order < 2, order, chip + 2 - order)
-        slot = (chip - back) * CORES + jnp.where(own_core, core, other)
+        slot = (chip - turn // 2) * CORES + jnp.where(own_core, core, other)
         landed = held.at[slot]
         side_copy(landed, slot).wait_recv()
 
-        @pl.when(jnp.logical_and(own_core, jnp.logical_and(chip < chips - 1, back < reach)))
+        @pl.when(jnp.logical_and(own_core, chip < chips - 1))
         def _():
             up_copy(landed, slot).start()
 
@@ -261,7 +246,7 @@
     def finish(step):
         slot = (chip - step) * CORES + core
 
-        @pl.when(jnp.logical_and(chip < chips - 1, step < reach))
+        @pl.when(chip < chips - 1)
         def _():
             up_copy(held.at[slot], slot).wait_send()
 
@@ -270,7 +255,6 @@
             side_copy(held.at[slot], slot).wait_send()
 
     loop(chip + 1, finish)
-    loop(far_count, lambda turn: far_copy(chips - 1 - turn).wait_send())
 
     @pl.when(core == 0)
     def _():

time: 184 us -> 185 us (level)
  starting transfers between devices: 39.6 us -> 44.7 us
  Pallas kernels: 98.6 us -> 94.3 us
    pallas_call x1, Pallas kernels: 55.4 us -> 50 us  [attention(): pl.pallas_call(functools.partial(attention_kernel, heads), out_shape=[jax...]
    all_to_all x1, starting transfers between devices: 39.6 us -> 44.7 us  [local(): lax.all_to_all(result, 'ep', split_axis=0, concat_axis=0, tiled=True)]
where the time goes in v4:
time: 185 us; the launch traced here: 184 us
  Pallas kernels  94.3 us (51%)
  starting transfers between devices  44.7 us (24%)
  matrix products  21.8 us (12%)
  local copies, waits for them, and re-layouts  14.8 us (8%)
  other arithmetic  7.29 us (4%)
    pallas_call x1, Pallas kernels, attention(): pl.pallas_call(functools.partial(attention_kernel, heads), out_shape=[jax...  50 us
    all_to_all x1, starting transfers between devices, local(): lax.all_to_all(result, 'ep', split_axis=0, concat_axis=0, tiled=True)  44.7 us
    pallas_call x2, Pallas kernels, exchange(): pl.pallas_call(functools.partial(exchange_kernel, count), out_shape=[gath...  44.4 us
    convert_element_type x2, local copies, waits for them, and re-layouts, local(): spread = jnp.where(place, weight[:, :, None], 0.0).astype(jnp.bfloat16)  4.24 us
    dot_general x1, matrix products, local(): jnp.einsum('ast,atd->asd', pick, tokens, preferred_element_type=jnp.float32)  4.17 us
  transfers between devices with their start and end apart: 1, of which 0 were waited for; matrix products, arithmetic and copies ran while one was open for 5% of the time, Pallas kernels for 13%

profile of v4, /device:TPU:0, one launch (start us, length us, event | category | flops | bytes accessed | tf_op | source)
XLA Modules:
  0.0 183.9 jit_solution(1489984076882784015)
XLA Ops:
  0.6 0.0 copy-start
  0.6 0.0 copy-start.3
  0.8 1.2 broadcast_multiply_fusion
  2.0 1.0 reduce-precision_convert_fusion.1
  2.9 0.0 copy-done.3
  2.9 0.2 fusion.4
  3.2 0.2 fusion.16
  3.4 1.4 fusion.6.normed_ref
  4.8 1.2 pad_maximum_fusion.1.kv_ref
  6.0 0.1 broadcast_select_fusion.3
  6.1 0.2 maximum_bitcast_fusion
  6.3 0.2 pad_maximum_fusion.q_ref
  6.5 2.8 %convolution_convert_fusion.gate_ref = bf16[6144,256]{1,0:T(8,128)(2,1)} fusion(bf16[4,6144]{1,0:T(4,128)(2,1)S(1)} %get-tuple-element.23, bf16[4,6144]{1,0:T(4,128)(2,1)S(1)} %get-tuple-element.24, bf16[4,6144]{1,0:T(4,128)(2,1)S(1)} %get-tuple-element.22, s32[12]{0:T(128)S(1)} %fusion.25), kind=kOutput, calls=%fused_computation | convolution fusion | flops 39767040 | bytes 3293232 | tf_op jit(solution)/shard_map/dot_general | solution.py:389
  9.2 50.0 %attend.1 = (bf16[768,256]{1,0:T(8,128)(2,1)S(1)}, bf16[8,192,2048]{2,1,0:T(8,128)(2,1)}, bf16[8,4,192]{2,1,0:T(4,128)(2,1)S(1)}) custom-call(bf16[4,768,256]{2,1,0:T(8,128)(2,1)S(1)} %pad_maximum_fusion.q_ref, bf16[768,512]{1,0:T(8,128)(2,1)S(1)} %pad_maximum_fusion.1.kv_ref, bf16[6144,256]{1,0:T(8,128)(2,1)} %convolution_convert_fusion.gate_ref, ...), custom_call_target="tpu_custom_call" | custom-call | flops 19327352832 | bytes 8388608 | tf_op jit(solution)/shard_map/attend/pallas_call | solution.py:393
  59.2 0.8 copy-done.1
  60.0 0.1 eq.124
  60.1 0.3 bitcast_compare_fusion
  60.3 4.2 %convolution_convert_fusion.1 = bf16[8,144,2048]{2,1,0:T(8,128)(2,1)S(1)} fusion(bf16[8,192,2048]{2,1,0:T(8,128)(2,1)} %get-tuple-element.10, pred[8,144,192]{2,0,1:T(8,128)(4,1)S(1)} %bitcast_compare_fusion), kind=kOutput, calls=%fused_computation.1 | convolution fusion | flops 908328960 | bytes 11231232 | tf_op jit(solution)/shard_map/ast,atd->asd/dot_general | solution.py:479
  64.5 0.0 copy-start.2
  64.5 2.6 %copy.33 = bf16[8,144,2048]{2,0,1:T(8,128)(2,1)S(1)} copy(bf16[8,144,2048]{2,1,0:T(8,128)(2,1)S(1)} %convolution_convert_fusion.1) | data formatting | bytes 9437184 | tf_op jit(solution)/shard_map/convert_element_type | solution.py:480
  67.1 0.0 copy-done.2
  67.1 0.0 copy-start.10
  67.1 1.4 fusion.2
  68.5 0.2 copy-done.10
  68.7 1.4 fusion.10
  70.1 0.1 copy.34
  70.2 0.8 reshape.191.refs_0_
  71.0 1.4 fusion.29
  72.4 2.0 %fusion.15.refs_1_ = bf16[192,128]{1,0:T(8,128)(2,1)} fusion(bf16[192,2048]{1,0:T(8,128)(2,1)S(1)} %fusion.6.normed_ref, bf16[2048,128]{1,0:T(8,128)(2,1)} %param.28, f32[192,128]{1,0:T(8,128)S(1)} %fusion.29), kind=kOutput, calls=%fused_computation.24 | convolution fusion | flops 100810752 | bytes 1458176 | tf_op jit(solution)/shard_map/dot_general | solution.py:488
  74.4 21.2 %exchange.2 = (bf16[1152,512]{1,0:T(8,128)(2,1)}, bf16[192,512]{1,0:T(8,128)(2,1)}) custom-call(bf16[1152,128]{1,0:T(8,128)(2,1)} %reshape.191.refs_0_, bf16[192,128]{1,0:T(8,128)(2,1)} %fusion.15.refs_1_), custom_call_target="tpu_custom_call" | custom-call | bytes 25165824 | tf_op jit(solution)/shard_map/exchange/pallas_call | solution.py:339
  95.6 2.0 %convolution_convert_fusion.2 = bf16[4,288,512]{2,1,0:T(8,128)(2,1)S(1)} fusion(bf16[4,288,512]{2,1,0:T(8,128)(2,1)} %bitcast.56, bf16[4,512,512]{2,1,0:T(8,128)(2,1)S(1)} %copy-done), kind=kOutput, calls=%fused_computation.12 | convolution fusion | flops 604569600 | bytes 4456448 | tf_op jit(solution)/shard_map/esf,efd->esd/dot_general | solution.py:494
  97.7 1.9 %copy.35 = bf16[4,288,512]{2,0,1:T(4,128)(2,1)} copy(bf16[4,288,512]{2,1,0:T(8,128)(2,1)S(1)} %convolution_convert_fusion.2) | data formatting | bytes 2359296 | tf_op jit(solution)/shard_map/convert_element_type | solution.py:495
  99.6 44.7 %all-to-all-start = ((bf16[8,4,36,512]{3,1,2,0:T(4,128)(2,1)}), bf16[8,4,36,512]{3,1,2,0:T(4,128)(2,1)S(1)}, u32[]{:S(2)}, u32[]{:S(2)}) async-start(bf16[8,4,36,512]{3,1,2,0:T(4,128)(2,1)} %bitcast.55), calls=%async_computation | async-start | bytes 2359296 | tf_op jit(solution)/shard_map/all_to_all | solution.py:498
  144.3 1.5 select_convert_fusion
  145.9 2.1 %convert_element_type.110 = bf16[192,1152]{0,1:T(8,128)(2,1)} reshape(bf16[192,32,36]{0,2,1:T(8,128)(2,1)} %get-tuple-element.26) | data formatting | bytes 884736 | tf_op jit(solution)/shard_map/convert_element_type | solution.py:504
  148.0 2.1 %convert_element_type.112 = bf16[192,1152]{0,1:T(8,128)(2,1)} reshape(bf16[192,32,36]{0,2,1:T(8,128)(2,1)} %get-tuple-element.25) | data formatting | bytes 884736 | tf_op jit(solution)/shard_map/convert_element_type | solution.py:504
  150.1 23.1 %exchange.3 = bf16[768,1024]{1,0:T(8,128)(2,1)} custom-call(bf16[768,256]{1,0:T(8,128)(2,1)} %copy-done.1), custom_call_target="tpu_custom_call" | custom-call | bytes 25165824 | tf_op jit(solution)/shard_map/exchange/pallas_call | solution.py:339
  173.2 3.6 %convolution_convert_fusion.3 = bf16[768,512]{1,0:T(8,128)(2,1)} fusion(bf16[768,1024]{1,0:T(8,128)(2,1)} %exchange.3, bf16[1024,512]{1,0:T(8,128)(2,1)} %param.19), kind=kOutput, calls=%fused_computation.13 | convolution fusion | flops 805699584 | bytes 3407872 | tf_op jit(solution)/shard_map/dot_general | solution.py:511
  176.8 0.0 all-to-all-done
  176.8 1.4 copy.36
  178.2 2.1 %reshape.194 = bf16[1152,512]{1,0:T(8,128)(2,1)S(1)} reshape(bf16[8,4,36,512]{3,2,1,0:T(8,128)(2,1)} %copy.36) | data formatting | bytes 2359296 | tf_op jit(solution)/shard_map/reshape | solution.py:499
  180.3 1.6 fusion.30
  181.9 0.0 copy-start.5
  181.9 0.0 copy-start.6
  181.9 0.5 convolution_add_fusion.1
  182.4 0.6 copy-done.5
  183.0 0.0 copy-done.6
  183.0 0.9 fusion.14
  (26 shorter events, 0.2 us)
Async XLA Ops:
  0.6 95.0 %copy-start = (bf16[4,512,512]{2,1,0:T(8,128)(2,1)S(1)}, bf16[4,512,512]{2,1,0:T(8,128)(2,1)}, u32[]{:S(2)}) copy-start(bf16[4,512,512]{2,1,0:T(8,128)(2,1)} %param.26) | copy-start | bytes 6291460
  0.6 2.3 %copy-start.3 = (bf16[192,2048]{1,0:T(8,128)(2,1)S(1)}, bf16[192,2048]{1,0:T(8,128)(2,1)}, u32[]{:S(2)}) copy-start(bf16[192,2048]{1,0:T(8,128)(2,1)} %param.20) | copy-start | bytes 2359300
  0.7 2.5 %copy-start.7 = (s32[192,3]{0,1:T(4,128)S(1)}, s32[192,3]{0,1:T(4,128)}, u32[]{:S(2)}) copy-start(s32[192,3]{0,1:T(4,128)} %param.22) | copy-start | bytes 6916
  0.7 2.8 %copy-start.8 = (f32[2048]{0:T(1024)S(1)}, f32[2048]{0:T(1024)}, u32[]{:S(2)}) copy-start(f32[2048]{0:T(1024)} %param.21) | copy-start | bytes 24580
  59.2 0.8 copy-start.1
  64.5 2.6 %copy-start.2 = (bf16[4,2048,128]{2,1,0:T(8,128)(2,1)S(1)}, bf16[4,2048,128]{2,1,0:T(8,128)(2,1)}, u32[]{:S(2)}) copy-start(bf16[4,2048,128]{2,1,0:T(8,128)(2,1)} %param.24) | copy-start | bytes 6291460
  67.1 1.6 copy-start.10
  99.6 44.7 %copy-start.9 = (f32[192,3]{0,1:T(4,128)S(1)}, f32[192,3]{0,1:T(4,128)}, u32[]{:S(2)}) copy-start(f32[192,3]{0,1:T(4,128)} %param.23) | copy-start | bytes 6916
  99.6 77.2 %all-to-all-start = ((bf16[8,4,36,512]{3,1,2,0:T(4,128)(2,1)}), bf16[8,4,36,512]{3,1,2,0:T(4,128)(2,1)S(1)}, u32[]{:S(2)}, u32[]{:S(2)}) async-start(bf16[8,4,36,512]{3,1,2,0:T(4,128)(2,1)} %bitcast.55), calls=%async_computation | async-start | bytes 2359296 | tf_op jit(solution)/shard_map/all_to_all | solution.py:498
  180.3 1.6 copy-start.4
  181.9 1.0 copy-start.5
  181.9 1.1 copy-start.6
